TPU v7x, 32 devices: a whole 2x2x4 slice. The times are simulated.
32 devices in a mesh: sp: 8 (over z, x), tp: 4 (over y, core).
Axes of the slice: x: 2, y: 2, z: 4, core: 2. Of those that a mesh axis runs over, the one named last changes fastest.
Arguments:
- queries: bfloat16 [2560, 1024], P('sp', 'tp'), may hold values from -6.6 to 6.6
- key_matrix: bfloat16 [2560, 256], P('sp', 'tp'), may hold values from -6.6 to 6.6
- values: bfloat16 [2560, 256], P('sp', 'tp'), may hold values from -6 to 6
- query_gain: float32 [64], replicated, may hold values from 0.19 to 8
- key_norm_gain: float32 [64], replicated, may hold values from 0.19 to 8
- head_gain: float32 [1024], P('tp'), may hold values from 0.1 to 1.9
- out_proj: bfloat16 [1024, 2048], replicated, may hold values from -0.1875 to 0.1875
- residual: bfloat16 [2560, 2048], P('sp'), may hold values from -6 to 6
- ffn_gain: float32 [2048], replicated, may hold values from 0.1 to 1.9
- routes: int32 [2560, 4], P('sp'), may hold values from 0 to 31, all different within a row; in each aligned block of 320 rows (0 to 319, 320 to 639, ...) at most 80 rows name the same one
- route_weights: float32 [2560, 4], P('sp'), may hold values from 0.2 to 1
- expert_gate: bfloat16 [32, 2048, 512], P(('sp', 'tp')), may hold values from -0.125 to 0.125
- expert_up: bfloat16 [32, 2048, 512], P(('sp', 'tp')), may hold values from -0.125 to 0.125
- expert_down: bfloat16 [32, 512, 2048], P(('sp', 'tp')), may hold values from -0.25 to 0.25
- shared_gate: bfloat16 [2048, 512], P(None, 'tp'), may hold values from -0.125 to 0.125
- shared_up: bfloat16 [2048, 512], P(None, 'tp'), may hold values from -0.125 to 0.125
- shared_down: bfloat16 [512, 2048], P('tp'), may hold values from -0.25 to 0.25
Outputs:
- layer_out: bfloat16 [2560, 2048], P(('sp', 'tp'))
Inputs may be any that keep to these rules, and one draw needn't show every extreme that they name: `routes`: each row names 4 different experts; in each aligned block of 320 rows (the tokens of one index of sp) no expert is named more than 80 times, a bound that some block reaches.
All inputs are finite; a program needn't handle non-finite values.
Results may differ from a plain program's by a relative error of at most 0.019.
The roundings to bfloat16 on the way count: a program that leaves them out, or rounds other values in their place, can miss the bound.
Values may be sent and summed in bfloat16 or wider, within the bound.
A program may use at most 128 MiB of HBM per device.

v0:
```python
import jax
import jax.numpy as jnp
from jax import lax
from jax.sharding import PartitionSpec as P

HEAD_SIZE = 64
GRID_W = 64


EPS = 1e-06
THETA = 10000.0


def final_norm(field, gain):
    mean_sq = jnp.mean(field * field, axis=-1, keepdims=True)
    return field * lax.rsqrt(mean_sq + EPS) * gain


def grid_tables(positions, sequence_total):
    grid_rows = sequence_total // GRID_W
    row_pos = (positions // GRID_W - grid_rows // 2).astype(jnp.float32)
    col_pos = (positions % GRID_W - GRID_W // 2).astype(jnp.float32)
    quarter = HEAD_SIZE // 4
    inverse = THETA ** (-jnp.arange(quarter, dtype=jnp.float32) / quarter)
    angles = jnp.concatenate([row_pos[:, None] * inverse, col_pos[:, None] * inverse], axis=1)
    return (jnp.cos(angles), jnp.sin(angles))


def apply_rotary(field, cosine_table, sine_table):
    row_count, head_count = (field.shape[0], field.shape[1])
    quarter = HEAD_SIZE // 4
    pieces = field.reshape(row_count, head_count, 2, 2, quarter)
    front_half = pieces[:, :, :, 0, :].reshape(row_count, head_count, 2 * quarter)
    back_half = pieces[:, :, :, 1, :].reshape(row_count, head_count, 2 * quarter)
    cos_wide = cosine_table[:, None, :]
    sin_wide = sine_table[:, None, :]
    new_front = (front_half * cos_wide - back_half * sin_wide).reshape(
        row_count, head_count, 2, 1, quarter
    )
    new_back = (front_half * sin_wide + back_half * cos_wide).reshape(
        row_count, head_count, 2, 1, quarter
    )
    return jnp.concatenate([new_front, new_back], axis=3).reshape(row_count, head_count, HEAD_SIZE)


def key_block_rows(piece_rows):
    return max((width for width in range(1, 2049) if piece_rows % width == 0))


def local(
    queries,
    key_matrix,
    values,
    query_gain,
    key_norm_gain,
    head_gain,
    out_proj,
    residual,
    ffn_gain,
    routes,
    route_weights,
    expert_gate,
    expert_up,
    expert_down,
    shared_gate,
    shared_up,
    shared_down,
):
    tok_count = queries.shape[0]
    head_count = queries.shape[1] // HEAD_SIZE
    sp_count = lax.axis_size("sp")
    tp_count = lax.axis_size("tp")
    tp_index = lax.axis_index("tp")
    sequence_total = tok_count * sp_count
    positions = lax.axis_index("sp") * tok_count + jnp.arange(tok_count, dtype=jnp.int32)
    cosine_table, sine_table = grid_tables(positions, sequence_total)
    rotated_query = apply_rotary(
        final_norm(
            queries.astype(jnp.float32).reshape(tok_count, head_count, HEAD_SIZE), query_gain
        ),
        cosine_table,
        sine_table,
    ).astype(jnp.bfloat16)
    rotated_key = (
        apply_rotary(
            final_norm(
                key_matrix.astype(jnp.float32).reshape(tok_count, 1, HEAD_SIZE), key_norm_gain
            ),
            cosine_table,
            sine_table,
        )
        .reshape(tok_count, HEAD_SIZE)
        .astype(jnp.bfloat16)
    )
    packed = jnp.concatenate([rotated_key, values], axis=1)
    query_rows = rotated_query.transpose(1, 0, 2).reshape(head_count * tok_count, HEAD_SIZE)
    score_scale = HEAD_SIZE ** (-0.5)
    start_state = (
        jnp.full((head_count * tok_count,), -1e30, jnp.float32),
        jnp.zeros((head_count * tok_count,), jnp.float32),
        jnp.zeros((head_count * tok_count, HEAD_SIZE), jnp.float32),
    )
    state = start_state
    piece = lax.all_gather(packed, "sp", axis=0, tiled=True)
    piece_rows = piece.shape[0]
    block_length = key_block_rows(piece_rows)
    key_blocks = piece.reshape(piece_rows // block_length, block_length, 2 * HEAD_SIZE)

    def step(carry, key_slab):
        run_max, run_total, run_acc = carry
        scores = (
            lax.dot_general(
                query_rows,
                key_slab[:, :HEAD_SIZE],
                (((1,), (1,)), ((), ())),
                preferred_element_type=jnp.float32,
            )
            * score_scale
        )
        new_max = jnp.maximum(run_max, jnp.max(scores, axis=1))
        factor = jnp.exp(run_max - new_max)
        expo_terms = jnp.exp(scores - new_max[:, None])
        new_total = run_total * factor + jnp.sum(expo_terms, axis=1)
        new_acc = run_acc * factor[:, None] + jnp.dot(
            expo_terms.astype(jnp.bfloat16),
            key_slab[:, HEAD_SIZE:],
            preferred_element_type=jnp.float32,
        )
        return ((new_max, new_total, new_acc), None)

    state, _ = lax.scan(step, state, key_blocks)
    run_max, run_total, run_acc = state
    attended = (
        (run_acc / run_total[:, None]).reshape(head_count, tok_count, HEAD_SIZE).transpose(1, 0, 2)
    )
    head_out = final_norm(attended, head_gain.reshape(head_count, HEAD_SIZE)).astype(jnp.bfloat16)
    head_out = head_out.reshape(tok_count, head_count * HEAD_SIZE)
    part_rows = tok_count // tp_count
    token_heads = lax.all_to_all(head_out, "tp", split_axis=0, concat_axis=1, tiled=True)
    own_resid = lax.dynamic_slice_in_dim(residual, tp_index * part_rows, part_rows, 0)
    hidden_own = (
        own_resid.astype(jnp.float32)
        + jnp.dot(token_heads, out_proj, preferred_element_type=jnp.float32)
    ).astype(jnp.bfloat16)
    normed_own = final_norm(hidden_own.astype(jnp.float32), ffn_gain).astype(jnp.bfloat16)
    normed = lax.all_gather(normed_own, "tp", axis=0, tiled=True)
    model_width = normed.shape[1]
    topk_count = routes.shape[1]
    capacity = max(2, 2 * tok_count * topk_count // (sp_count * tp_count))
    slot_total = sp_count * capacity
    flat_expert = routes.reshape(-1)
    entry_token = jnp.arange(tok_count * topk_count, dtype=jnp.int32) // topk_count
    is_mine = flat_expert % tp_count == tp_index
    target = flat_expert // tp_count
    onehot = (target[:, None] == jnp.arange(sp_count, dtype=jnp.int32)[None, :]) & is_mine[:, None]
    running = jnp.cumsum(onehot.astype(jnp.int32), axis=0) - 1
    rank_own = jnp.sum(jnp.where(onehot, running, 0), axis=1)
    slot = jnp.where(is_mine, target * capacity + rank_own, slot_total)
    slot_token = jnp.zeros((slot_total,), jnp.int32).at[slot].set(entry_token, mode="drop")
    filled = jnp.zeros((slot_total,), jnp.bool_).at[slot].set(True, mode="drop")
    outgoing = jnp.where(
        filled[:, None], jnp.take(normed, slot_token, axis=0), jnp.zeros((), jnp.bfloat16)
    )
    outgoing = outgoing.reshape(sp_count, capacity, model_width)
    gate_local = expert_gate[0]
    up_local = expert_up[0]
    down_local = expert_down[0]
    arrived = lax.all_to_all(outgoing, "sp", split_axis=0, concat_axis=0, tiled=True)
    source_count, slot_count, width_in = arrived.shape
    flat_rows = arrived.reshape(source_count * slot_count, width_in)
    gate_out = jnp.dot(flat_rows, gate_local, preferred_element_type=jnp.float32)
    up_out = jnp.dot(flat_rows, up_local, preferred_element_type=jnp.float32)
    expert_inner = (jax.nn.silu(gate_out) * up_out).astype(jnp.bfloat16)
    produced = jnp.dot(expert_inner, down_local, preferred_element_type=jnp.float32).astype(
        jnp.bfloat16
    )
    produced = produced.reshape(source_count, slot_count, width_in)
    returned = lax.all_to_all(produced, "sp", split_axis=0, concat_axis=0, tiled=True).reshape(
        slot_total, model_width
    )
    entry_slot = jnp.minimum(slot, slot_total - 1)
    selected = jnp.take(returned, entry_slot, axis=0).astype(jnp.float32)
    entry_scale = jnp.where(is_mine, route_weights.reshape(-1), 0.0)
    routed = (
        (selected * entry_scale[:, None]).reshape(tok_count, topk_count, model_width).sum(axis=1)
    )
    gate_part = jnp.dot(normed, shared_gate, preferred_element_type=jnp.float32)
    up_part = jnp.dot(normed, shared_up, preferred_element_type=jnp.float32)
    shared_inner = (jax.nn.silu(gate_part) * up_part).astype(jnp.bfloat16)
    mixed_rows = lax.psum_scatter(
        (jnp.dot(shared_inner, shared_down, preferred_element_type=jnp.float32) + routed).astype(
            jnp.bfloat16
        ),
        "tp",
        scatter_dimension=0,
        tiled=True,
    ).astype(jnp.float32)
    return (hidden_own.astype(jnp.float32) + mixed_rows).astype(jnp.bfloat16)


def solution(mesh):
    placed = (
        P("sp", "tp"),
        P("sp", "tp"),
        P("sp", "tp"),
        P(),
        P(),
        P("tp"),
        P(),
        P("sp", None),
        P(),
        P("sp", None),
        P("sp", None),
        P(("sp", "tp"), None, None),
        P(("sp", "tp"), None, None),
        P(("sp", "tp"), None, None),
        P(None, "tp"),
        P(None, "tp"),
        P("tp", None),
    )
    return jax.shard_map(
        local, mesh=mesh, in_specs=placed, out_specs=P(("sp", "tp"), None), check_vma=False
    )
```

profile of v0, /device:TPU:13, one launch (start us, length us, event | category | flops | bytes accessed | tf_op | source)
XLA Modules:
  0.0 321.3 jit_solution(6801265648340296357)
XLA Ops:
  6.6 1.2 copy.81
  7.9 0.7 mul.292
  8.7 0.2 fusion.53
  9.1 0.2 copy.98
  9.5 0.2 subtract_convert_fusion.1
  9.9 25.5 %all_gather.6 = bf16[2560,128]{1,0:T(8,128)(2,1)} all-gather(bf16[320,128]{1,0:T(8,128)(2,1)S(1)} %copy.80), channel_id=1, replica_groups=mesh['sp'=8,'tp'=4] {'sp'}, dimensions={0}, use_global_device_ids=true | all-gather | bytes 737280 | tf_op jit(solution)/shard_map/all_gather | solution.py:104
  35.3 21.4 %while.15 = (s32[]{:T(128)}, f32[1280]{0:T(1024)S(1)}, f32[1280]{0:T(1024)S(1)}, f32[1280,64]{0,1:T(8,128)S(1)}, bf16[2,1280,128]{2,1,0:T(8,128)(2,1)}, /*index=5*/bf16[1280,64]{1,0:T(8,128)(2,1)S(1)}, s32[]{:T(128)}, s32[]{:T(128)}) while((s32[]{:T(128)}, f32[1280]{0:T(1024)S(1)}, f32[1280]{0:T(1024)S(1)}, ...), condition=%wide.region_5.6_spmd.clone, body=%wide.region_2.5_spmd.clone.sunk | while | flops 429512960 | bytes 48087168 | solution.py:131
  35.3 1.0 dynamic-slice_bitcast_fusion.2
  36.4 3.8 %fusion.104 = (f32[1280]{0:T(1024)S(1)}, f32[1280,1280]{1,0:T(8,128)}) fusion(bf16[1280,64]{1,0:T(8,128)(2,1)S(1)} %get-tuple-element.179, bf16[1280,128]{1,0:T(8,128)(2,1)S(1)} %dynamic-slice_bitcast_fusion.2), kind=kOutput, calls=%fused_computation.167.clone.1 | convolution fusion | flops 212990720 | bytes 7050240 | tf_op jit(solution)/shard_map/while/body/eval_jaxpr/dot_general | solution.py:112
  40.1 3.9 %fusion.105 = f32[1280]{0:T(1024)S(1)} fusion(f32[1280,1280]{1,0:T(8,128)} %get-tuple-element.155, f32[1280]{0:T(1024)S(1)} %select_maximum_fusion.2), kind=kLoop, calls=%fused_computation.7.clone.1 | loop fusion | flops 3275520 | bytes 6563840 | tf_op jit(solution)/shard_map/while/body/eval_jaxpr/reduce_sum | solution.py:123
  44.1 0.8 copy-done.1
  44.9 1.2 fusion.107
  46.1 1.0 dynamic-slice_bitcast_fusion.2
  47.1 3.8 %fusion.104 = (f32[1280]{0:T(1024)S(1)}, f32[1280,1280]{1,0:T(8,128)}) fusion(bf16[1280,64]{1,0:T(8,128)(2,1)S(1)} %get-tuple-element.179, bf16[1280,128]{1,0:T(8,128)(2,1)S(1)} %dynamic-slice_bitcast_fusion.2), kind=kOutput, calls=%fused_computation.167.clone.1 | convolution fusion | flops 212990720 | bytes 7050240 | tf_op jit(solution)/shard_map/while/body/eval_jaxpr/dot_general | solution.py:112
  50.8 3.9 %fusion.105 = f32[1280]{0:T(1024)S(1)} fusion(f32[1280,1280]{1,0:T(8,128)} %get-tuple-element.155, f32[1280]{0:T(1024)S(1)} %select_maximum_fusion.2), kind=kLoop, calls=%fused_computation.7.clone.1 | loop fusion | flops 3275520 | bytes 6563840 | tf_op jit(solution)/shard_map/while/body/eval_jaxpr/reduce_sum | solution.py:123
  54.8 0.8 copy-done.1
  55.6 1.2 fusion.107
  56.8 0.3 reshape.643
  57.6 0.8 copy.85
  58.4 10.1 %all-to-all-start = ((bf16[4,80,256]{2,1,0:T(8,128)(2,1)}), bf16[4,80,256]{2,1,0:T(8,128)(2,1)S(1)}, u32[]{:S(2)}, u32[]{:S(2)}) async-start(bf16[4,80,256]{2,1,0:T(8,128)(2,1)} %copy.85), calls=%async_computation | async-start | bytes 327680 | tf_op jit(solution)/shard_map/all_to_all | solution.py:139
  68.8 2.8 all-to-all-done
  71.6 3.2 %multiply_reduce_fusion.1 = (f32[80]{0:T(128)S(1)}, f32[80,2048]{1,0:T(8,128)S(1)}) fusion(bf16[80,1024]{1,0:T(8,128)(2,1)S(1)} %bitcast.91, bf16[1024,2048]{1,0:T(8,128)(2,1)} %param.25, bf16[320,2048]{1,0:T(8,128)(2,1)} %param.26, s32[]{:T(128)S(6)} %select_n.167), kind=kOutput, calls=%fused_computation.39 | convolution fusion | flops 336527296 | bytes 5341508 | tf_op jit(solution)/shard_map/dot_general | solution.py:143
  74.9 0.9 copy-done.4
  75.7 0.8 multiply_convert_fusion
  76.9 2.3 reduce-window.6
  79.2 0.3 slice_reduce_fusion
  79.9 5.4 %scatter_custom_fusion.1 = s32[640]{0:T(1024)S(1)} fusion(s32[1280]{0:T(1024)S(1)} %get-tuple-element.80, s32[1280]{0:T(1024)S(1)} %add_select_fusion.2, s32[]{:T(128)} %constant.142.clone.1), kind=kCustom, calls=%fused_computation.153 | custom fusion | bytes 2564 | tf_op jit(solution)/shard_map/scatter | solution.py:159
  85.5 11.2 %scatter_custom_fusion = pred[640]{0:T(1024)(128)(4,1)S(1)} fusion(s32[1280]{0:T(1024)S(1)} %get-tuple-element.80, pred[1280]{0:T(1024)(128)(4,1)S(1)} %broadcast.667, pred[]{:T(512)} %constant.166.clone.1), kind=kCustom, calls=%fused_computation.160 | custom fusion | bytes 641 | tf_op jit(solution)/shard_map/scatter | solution.py:160
  96.8 1.3 all-gather.2.cloned.1.call-done
  98.1 8.4 %gather_fusion = bf16[640,2048]{1,0:T(8,128)(2,1)} fusion(bf16[320,2048]{1,0:T(8,128)(2,1)} %all-gather.2.cloned.1.call-done, s32[1024]{0:T(1024)S(1)} %pad_clamp_fusion.1), kind=kCustom, calls=%fused_computation | custom fusion | bytes 5245440 | tf_op jit(solution)/shard_map/jit(_take)/gather | solution.py:162
  106.5 2.1 select_select_fusion
  108.7 64.5 %all_to_all.29 = bf16[8,80,2048]{2,1,0:T(8,128)(2,1)S(1)} all-to-all(bf16[8,80,2048]{2,1,0:T(8,128)(2,1)S(1)} %select_select_fusion), channel_id=1, replica_groups=mesh['sp'=8,'tp'=4] {'sp'}, dimensions={0} | all-to-all | bytes 5242880 | tf_op jit(solution)/shard_map/all_to_all | solution.py:168
  173.2 1.5 copy-done.5
  174.7 1.5 fusion.17
  176.3 6.9 %convolution_convert_fusion = bf16[640,2048]{1,0:T(8,128)(2,1)} fusion(bf16[1,512,2048]{2,1,0:T(8,128)(2,1)S(1)} %copy-done, bf16[640,2048]{1,0:T(8,128)(2,1)} %bitcast.88, bf16[1,2048,512]{2,1,0:T(8,128)(2,1)} %param.31, f32[640,512]{1,0:T(8,128)S(1)} %fusion.17), kind=kOutput, calls=%fused_computation.20 | convolution fusion | flops 2687631360 | bytes 10747904 | tf_op jit(solution)/shard_map/dot_general | solution.py:174
  183.1 5.2 %all-to-all-start.2 = ((bf16[8,80,2048]{2,1,0:T(8,128)(2,1)}), bf16[8,80,2048]{2,1,0:T(8,128)(2,1)}, u32[]{:S(2)}, u32[]{:S(2)}) async-start(bf16[8,80,2048]{2,1,0:T(8,128)(2,1)} %bitcast.86), calls=%async_computation.2 | async-start | bytes 5242880 | tf_op jit(solution)/shard_map/all_to_all | solution.py:178
  188.4 0.8 reduce_sum.72
  189.4 0.8 copy.97
  190.2 1.2 compare_and_fusion
  191.4 1.7 broadcast_select_fusion
  193.2 2.2 fusion.83
  195.4 50.7 %all-to-all-done.2 = bf16[8,80,2048]{2,1,0:T(8,128)(2,1)} async-done(((bf16[8,80,2048]{2,1,0:T(8,128)(2,1)}), bf16[8,80,2048]{2,1,0:T(8,128)(2,1)}, u32[]{:S(2)}, u32[]{:S(2)}) %all-to-all-start.2) | async-done | bytes 2621472 | tf_op jit(solution)/shard_map/all_to_all | solution.py:178
  246.2 12.9 %gather_fusion.1 = bf16[1280,2048]{1,0:T(8,128)(2,1)} fusion(bf16[640,2048]{1,0:T(8,128)(2,1)} %bitcast.21, s32[2048]{0:T(1024)S(1)} %pad_clamp_fusion), kind=kCustom, calls=%fused_computation.1 | custom fusion | bytes 10490880 | tf_op jit(solution)/shard_map/jit(_take)/gather | solution.py:182
  259.1 8.7 %gather.15 = bf16[320,4,2048]{2,1,0:T(4,128)(2,1)} reshape(bf16[1280,2048]{1,0:T(8,128)(2,1)} %gather_fusion.1) | data formatting | bytes 10485760 | tf_op jit(solution)/shard_map/jit(_take)/gather | solution.py:182
  267.7 13.7 %multiply_reduce_fusion = f32[320,2048]{1,0:T(8,128)} fusion(f32[320,4]{1,0:T(8,128)} %broadcast_select_fusion, bf16[320,4,2048]{2,1,0:T(4,128)(2,1)} %gather.15, pred[320,4]{1,0:T(8,128)(4,1)S(1)} %compare_and_fusion), kind=kLoop, calls=%fused_computation.19 | loop fusion | flops 9830400 | bytes 7870720 | tf_op jit(solution)/shard_map/reduce_sum | solution.py:185
  281.4 4.8 %fusion.11 = bf16[320,2048]{1,0:T(8,128)(2,1)} fusion(f32[320,2048]{1,0:T(8,128)} %multiply_reduce_fusion, bf16[128,2048]{1,0:T(8,128)(2,1)} %param.35, bf16[320,2048]{1,0:T(8,128)(2,1)S(1)} %copy-done.2, bf16[2048,128]{1,0:T(8,128)(2,1)} %param.34, f32[320,128]{1,0:T(8,128)} %fusion.83), kind=kOutput, calls=%fused_computation.22 | convolution fusion | flops 337100800 | bytes 6455296 | tf_op jit(solution)/shard_map/dot_general | solution.py:191
  286.2 26.3 %reduce-scatter.2.cloned.1.call-done = bf16[80,2048]{1,0:T(8,128)(2,1)} async-done(((bf16[320,2048]{1,0:T(8,128)(2,1)}), bf16[80,2048]{1,0:T(8,128)(2,1)}) %reduce-scatter.2.cloned.1.call-update) | async-done | bytes 327696 | tf_op jit(solution)/shard_map/reduce_scatter | solution.py:190
  312.5 2.0 add_convert_fusion
  (84 shorter events, 2.6 us)
Async XLA Ops:
  6.5 169.7 %copy-start = (bf16[1,512,2048]{2,1,0:T(8,128)(2,1)S(1)}, bf16[1,512,2048]{2,1,0:T(8,128)(2,1)}, u32[]{:S(2)}) copy-start(bf16[1,512,2048]{2,1,0:T(8,128)(2,1)} %param.32) | copy-start | bytes 6291460
  6.5 2.8 copy-start.6
  6.5 2.9 copy-start.12
  6.5 3.2 copy-start.7
  35.3 21.8 %copy-start.11 = (f32[256]{0:T(256)S(1)}, f32[256]{0:T(256)}, u32[]{:S(2)}) copy-start(f32[256]{0:T(256)} %param.24) | copy-start | bytes 3076
  40.1 4.7 %copy-start.1 = (f32[1280,1280]{1,0:T(8,128)S(1)}, f32[1280,1280]{1,0:T(8,128)}, u32[]{:S(2)}) copy-start(f32[1280,1280]{1,0:T(8,128)} %get-tuple-element.155) | copy-start | bytes 19660804 | tf_op jit(solution)/shard_map/while
  50.8 4.7 %copy-start.1 = (f32[1280,1280]{1,0:T(8,128)S(1)}, f32[1280,1280]{1,0:T(8,128)}, u32[]{:S(2)}) copy-start(f32[1280,1280]{1,0:T(8,128)} %get-tuple-element.155) | copy-start | bytes 19660804 | tf_op jit(solution)/shard_map/while
  56.8 11.7 %copy-start.8 = (s32[320,4]{0,1:T(4,128)S(1)}, s32[320,4]{0,1:T(4,128)}, u32[]{:S(2)}) copy-start(s32[320,4]{0,1:T(4,128)} %param.28) | copy-start | bytes 15364
  58.4 13.2 %all-to-all-start = ((bf16[4,80,256]{2,1,0:T(8,128)(2,1)}), bf16[4,80,256]{2,1,0:T(8,128)(2,1)S(1)}, u32[]{:S(2)}, u32[]{:S(2)}) async-start(bf16[4,80,256]{2,1,0:T(8,128)(2,1)} %copy.85), calls=%async_computation | async-start | bytes 327680 | tf_op jit(solution)/shard_map/all_to_all | solution.py:139
  68.5 29.6 %all-gather.2.cloned.1.call-start = ((), (), s32[]{:S(2)}) async-start(), calls=%async_computation.4 | async-start | bytes 1638400 | tf_op jit(solution)/shard_map/all_gather | solution.py:146
  68.6 8.1 %copy-start.3 = (s32[320,4]{1,0:T(8,128)}, s32[320,4]{1,0:T(8,128)S(1)}, u32[]{:S(2)}) copy-start(s32[320,4]{1,0:T(8,128)S(1)} %copy.88) | copy-start | bytes 15364
  71.6 4.1 %copy-start.9 = (f32[2048]{0:T(1024)S(1)}, f32[2048]{0:T(1024)}, u32[]{:S(2)}) copy-start(f32[2048]{0:T(1024)} %param.27) | copy-start | bytes 24580
  74.9 0.9 copy-start.4
  108.7 66.1 %copy-start.13 = (bf16[1,2048,512]{2,1,0:T(8,128)(2,1)S(1)}, bf16[1,2048,512]{2,1,0:T(8,128)(2,1)}, u32[]{:S(2)}) copy-start(bf16[1,2048,512]{2,1,0:T(8,128)(2,1)} %param.30) | copy-start | bytes 6291460
  173.2 1.5 copy-start.5
  183.1 6.3 %copy-start.10 = (f32[320,4]{0,1:T(4,128)S(1)}, f32[320,4]{0,1:T(4,128)}, u32[]{:S(2)}) copy-start(f32[320,4]{0,1:T(4,128)} %param.29) | copy-start | bytes 15364
  183.1 10.1 %copy-start.2 = (bf16[320,2048]{1,0:T(8,128)(2,1)S(1)}, bf16[320,2048]{1,0:T(8,128)(2,1)}, u32[]{:S(2)}) copy-start(bf16[320,2048]{1,0:T(8,128)(2,1)} %all-gather.2.cloned.1.call-done) | copy-start | bytes 3932164
  183.1 63.0 %all-to-all-start.2 = ((bf16[8,80,2048]{2,1,0:T(8,128)(2,1)}), bf16[8,80,2048]{2,1,0:T(8,128)(2,1)}, u32[]{:S(2)}, u32[]{:S(2)}) async-start(bf16[8,80,2048]{2,1,0:T(8,128)(2,1)} %bitcast.86), calls=%async_computation.2 | async-start | bytes 5242880 | tf_op jit(solution)/shard_map/all_to_all | solution.py:178
  188.4 124.2 %reduce-scatter.2.cloned.1.call-start = ((), (), s32[]{:S(2)}) async-start(), calls=%async_computation.5 | async-start | bytes 1638400 | tf_op jit(solution)/shard_map/reduce_scatter | solution.py:190
Sparse Core Ops, SparseCore 0:
  76.7 21.3 all-gather.1
  286.4 26.1 reduce-scatter.1
where the time goes:
time: 325 us; the launch traced here: 321 us
  blocking collectives  90 us (28%)
  waiting for transfers between devices  81.2 us (25%)
  local copies, waits for them, and re-layouts  59.1 us (18%)
  other arithmetic  33.4 us (10%)
  matrix products  28.5 us (9%)
  starting transfers between devices  15.3 us (5%)
  between operations  13.8 us (4%)
    all_to_all x1, blocking collectives, local(): lax.all_to_all(outgoing, 'sp', split_axis=0, concat_axis=0, tiled=True)  64.5 us
    all_to_all x1, waiting for transfers between devices, local(): lax.all_to_all(produced, 'sp', split_axis=0, concat_axis=0, tiled=True)  50.7 us
    reduce_scatter x1, waiting for transfers between devices, local(): lax.psum_scatter((jnp.dot(shared_inner, shared_down, preferred_element_ty...  26.3 us
    all_gather x1, blocking collectives, local(): piece = lax.all_gather(packed, 'sp', axis=0, tiled=True)  25.5 us
    gather x2, local copies, waits for them, and re-layouts, local(): selected = jnp.take(returned, entry_slot, axis=0).astype(jnp.float32)  21.6 us
    reduce_sum x1, other arithmetic, local(): (selected * entry_scale[:, None]).reshape(tok_count, topk_count, model_wi...  13.7 us
    scatter x1, local copies, waits for them, and re-layouts, local(): filled = jnp.zeros((slot_total,), jnp.bool_).at[slot].set(True, mode='drop')  11.2 us
    all_to_all x1, starting transfers between devices, local(): lax.all_to_all(head_out, 'tp', split_axis=0, concat_axis=1, tiled=True)  10.1 us
  transfers between devices with their start and end apart: 4, of which 4 were waited for; matrix products, arithmetic and copies ran while one was open for 9% of the time, Pallas kernels for 0%

commit v1 on v0

--- a/solution.py
+++ b/solution.py
@@ -1,6 +1,8 @@
 import jax
 import jax.numpy as jnp
 from jax import lax
+from jax.experimental import pallas as pl
+from jax.experimental.pallas import tpu as pltpu
 from jax.sharding import PartitionSpec as P
 
 HEAD_SIZE = 64
@@ -41,6 +43,57 @@
         row_count, head_count, 2, 1, quarter
     )
     return jnp.concatenate([new_front, new_back], axis=3).reshape(row_count, head_count, HEAD_SIZE)
+
+
+def exchange(block, axis, call_id, gather):
+    count = lax.axis_size(axis)
+    if count == 1:
+        return block[None] if gather else block
+    shape = (count,) + block.shape if gather else block.shape
+
+    def kernel(in_ref, out_ref, send_sems, recv_sems, own_sem):
+        me = lax.axis_index(axis)
+        barrier = pltpu.get_barrier_semaphore()
+        for step in range(1, count):
+            pl.semaphore_signal(
+                barrier,
+                inc=1,
+                device_id={axis: lax.rem(me + step, count)},
+                device_id_type=pl.DeviceIdType.MESH,
+            )
+        own = pltpu.make_async_copy(in_ref if gather else in_ref.at[me], out_ref.at[me], own_sem)
+        own.start()
+        pl.semaphore_wait(barrier, count - 1)
+        copies = []
+        for step in range(1, count):
+            peer = lax.rem(me + step, count)
+            copy = pltpu.make_async_remote_copy(
+                src_ref=in_ref if gather else in_ref.at[peer],
+                dst_ref=out_ref.at[me],
+                send_sem=send_sems.at[step],
+                recv_sem=recv_sems.at[step],
+                device_id={axis: peer},
+                device_id_type=pl.DeviceIdType.MESH,
+            )
+            copy.start()
+            copies.append(copy)
+        own.wait()
+        for copy in copies:
+            copy.wait()
+
+    return pl.pallas_call(
+        kernel,
+        out_shape=jax.ShapeDtypeStruct(shape, block.dtype),
+        in_specs=[pl.BlockSpec(memory_space=pltpu.VMEM)],
+        out_specs=pl.BlockSpec(memory_space=pltpu.VMEM),
+        scratch_shapes=[
+            pltpu.SemaphoreType.DMA((count,)),
+            pltpu.SemaphoreType.DMA((count,)),
+            pltpu.SemaphoreType.DMA,
+        ],
+        compiler_params=pltpu.CompilerParams(collective_id=call_id, has_side_effects=True),
+        name="exchange_%d" % call_id,
+    )(block)
 
 
 def key_block_rows(piece_rows):
@@ -101,7 +154,7 @@
         jnp.zeros((head_count * tok_count, HEAD_SIZE), jnp.float32),
     )
     state = start_state
-    piece = lax.all_gather(packed, "sp", axis=0, tiled=True)
+    piece = exchange(packed, "sp", 0, True).reshape(sequence_total, 2 * HEAD_SIZE)
     piece_rows = piece.shape[0]
     block_length = key_block_rows(piece_rows)
     key_blocks = piece.reshape(piece_rows // block_length, block_length, 2 * HEAD_SIZE)
@@ -136,65 +189,69 @@
     head_out = final_norm(attended, head_gain.reshape(head_count, HEAD_SIZE)).astype(jnp.bfloat16)
     head_out = head_out.reshape(tok_count, head_count * HEAD_SIZE)
     part_rows = tok_count // tp_count
-    token_heads = lax.all_to_all(head_out, "tp", split_axis=0, concat_axis=1, tiled=True)
+    token_heads = exchange(
+        head_out.reshape(tp_count, part_rows, head_count * HEAD_SIZE), "tp", 1, False
+    )
+    token_heads = token_heads.transpose(1, 0, 2).reshape(part_rows, -1)
     own_resid = lax.dynamic_slice_in_dim(residual, tp_index * part_rows, part_rows, 0)
     hidden_own = (
         own_resid.astype(jnp.float32)
         + jnp.dot(token_heads, out_proj, preferred_element_type=jnp.float32)
     ).astype(jnp.bfloat16)
     normed_own = final_norm(hidden_own.astype(jnp.float32), ffn_gain).astype(jnp.bfloat16)
-    normed = lax.all_gather(normed_own, "tp", axis=0, tiled=True)
-    model_width = normed.shape[1]
+    model_width = normed_own.shape[1]
+    normed = exchange(normed_own, "tp", 2, True).reshape(tok_count, model_width)
     topk_count = routes.shape[1]
     capacity = max(2, 2 * tok_count * topk_count // (sp_count * tp_count))
     slot_total = sp_count * capacity
-    flat_expert = routes.reshape(-1)
-    entry_token = jnp.arange(tok_count * topk_count, dtype=jnp.int32) // topk_count
-    is_mine = flat_expert % tp_count == tp_index
-    target = flat_expert // tp_count
-    onehot = (target[:, None] == jnp.arange(sp_count, dtype=jnp.int32)[None, :]) & is_mine[:, None]
-    running = jnp.cumsum(onehot.astype(jnp.int32), axis=0) - 1
-    rank_own = jnp.sum(jnp.where(onehot, running, 0), axis=1)
-    slot = jnp.where(is_mine, target * capacity + rank_own, slot_total)
-    slot_token = jnp.zeros((slot_total,), jnp.int32).at[slot].set(entry_token, mode="drop")
-    filled = jnp.zeros((slot_total,), jnp.bool_).at[slot].set(True, mode="drop")
-    outgoing = jnp.where(
-        filled[:, None], jnp.take(normed, slot_token, axis=0), jnp.zeros((), jnp.bfloat16)
-    )
-    outgoing = outgoing.reshape(sp_count, capacity, model_width)
+    experts_here = jnp.arange(sp_count, dtype=jnp.int32) * tp_count + tp_index
+    named = routes[:, :, None] == experts_here[None, None, :]
+    member = jnp.any(named, axis=1)
+    scale = jnp.sum(jnp.where(named, route_weights[:, :, None], 0.0), axis=1)
+    order = jnp.arange(tok_count, dtype=jnp.int32)
+    before = (order[:, None] > order[None, :]).astype(jnp.bfloat16)
+    rank = jnp.dot(
+        before, member.astype(jnp.bfloat16), preferred_element_type=jnp.float32
+    ).astype(jnp.int32)
+    rank = jnp.where(member, rank, -1)
+    slots = jnp.arange(capacity, dtype=jnp.int32)
+    chosen = rank.T[:, None, :] == slots[None, :, None]
+    select = chosen.astype(jnp.bfloat16).reshape(slot_total, tok_count)
+    outgoing = jnp.dot(select, normed, preferred_element_type=jnp.float32).astype(jnp.bfloat16)
     gate_local = expert_gate[0]
     up_local = expert_up[0]
     down_local = expert_down[0]
-    arrived = lax.all_to_all(outgoing, "sp", split_axis=0, concat_axis=0, tiled=True)
-    source_count, slot_count, width_in = arrived.shape
-    flat_rows = arrived.reshape(source_count * slot_count, width_in)
+    arrived = exchange(outgoing.reshape(sp_count, capacity, model_width), "sp", 3, False)
+    flat_rows = arrived.reshape(slot_total, model_width)
     gate_out = jnp.dot(flat_rows, gate_local, preferred_element_type=jnp.float32)
     up_out = jnp.dot(flat_rows, up_local, preferred_element_type=jnp.float32)
     expert_inner = (jax.nn.silu(gate_out) * up_out).astype(jnp.bfloat16)
     produced = jnp.dot(expert_inner, down_local, preferred_element_type=jnp.float32).astype(
         jnp.bfloat16
     )
-    produced = produced.reshape(source_count, slot_count, width_in)
-    returned = lax.all_to_all(produced, "sp", split_axis=0, concat_axis=0, tiled=True).reshape(
+    returned = exchange(produced.reshape(sp_count, capacity, model_width), "sp", 4, False).reshape(
         slot_total, model_width
     )
-    entry_slot = jnp.minimum(slot, slot_total - 1)
-    selected = jnp.take(returned, entry_slot, axis=0).astype(jnp.float32)
-    entry_scale = jnp.where(is_mine, route_weights.reshape(-1), 0.0)
-    routed = (
-        (selected * entry_scale[:, None]).reshape(tok_count, topk_count, model_width).sum(axis=1)
-    )
+    combine = jnp.where(chosen, scale.T[:, None, :], 0.0).reshape(slot_total, tok_count)
+    combine_hi = lax.reduce_precision(combine, 8, 7)
+    combine_lo = (combine - combine_hi).astype(jnp.bfloat16)
+    combine_hi = combine_hi.astype(jnp.bfloat16)
+
+    def mix(weights):
+        return lax.dot_general(
+            weights, returned, (((0,), (0,)), ((), ())), preferred_element_type=jnp.float32
+        )
+
     gate_part = jnp.dot(normed, shared_gate, preferred_element_type=jnp.float32)
     up_part = jnp.dot(normed, shared_up, preferred_element_type=jnp.float32)
     shared_inner = (jax.nn.silu(gate_part) * up_part).astype(jnp.bfloat16)
-    mixed_rows = lax.psum_scatter(
-        (jnp.dot(shared_inner, shared_down, preferred_element_type=jnp.float32) + routed).astype(
-            jnp.bfloat16
-        ),
-        "tp",
-        scatter_dimension=0,
-        tiled=True,
-    ).astype(jnp.float32)
+    shares = (
+        jnp.dot(shared_inner, shared_down, preferred_element_type=jnp.float32)
+        + mix(combine_hi)
+        + mix(combine_lo)
+    ).astype(jnp.bfloat16)
+    shares = exchange(shares.reshape(tp_count, part_rows, model_width), "tp", 5, False)
+    mixed_rows = jnp.sum(shares.astype(jnp.float32), axis=0)
     return (hidden_own.astype(jnp.float32) + mixed_rows).astype(jnp.bfloat16)
 
 

time: 325 us -> 260 us (0.80)
  Pallas kernels: 0 us -> 191 us
  blocking collectives: 90 us -> 0 us
  waiting for transfers between devices: 81.2 us -> 0 us
  local copies, waits for them, and re-layouts: 59.1 us -> 9.04 us
  other arithmetic: 33.4 us -> 13.4 us
  matrix products: 28.5 us -> 43.9 us
  starting transfers between devices: 15.3 us -> 0 us
  between operations: 13.8 us -> 0.33 us
    pallas_call x0 -> x6, Pallas kernels: none -> 191 us  [exchange(): pl.pallas_call(kernel, out_shape=jax.ShapeDtypeStruct(shape, block.dtype)...]
    all_to_all x1 -> x0, blocking collectives: 64.5 us -> none  [local(): lax.all_to_all(outgoing, 'sp', split_axis=0, concat_axis=0, tiled=True)]
    all_to_all x2 -> x0, waiting for transfers between devices: 53.5 us -> none  [the longest x1 50.7 us: local(): lax.all_to_all(produced, 'sp', split_axis=0, concat_axis=0, tiled=True)]
    gather x3 -> x0, local copies, waits for them, and re-layouts: 30 us -> none  [the longest x2 21.6 us: local(): selected = jnp.take(returned, entry_slot, axis=0).astype(jnp.float32)]
    reduce_scatter x1 -> x0, waiting for transfers between devices: 26.3 us -> none  [local(): lax.psum_scatter((jnp.dot(shared_inner, shared_down, preferred_element_ty...]
    all_gather x1 -> x0, blocking collectives: 25.5 us -> none  [local(): piece = lax.all_gather(packed, 'sp', axis=0, tiled=True)]
    scatter x2 -> x0, local copies, waits for them, and re-layouts: 16.6 us -> none  [the longest x1 11.2 us: local(): filled = jnp.zeros((slot_total,), jnp.bool_).at[slot].set(True, mode='drop')]
    all_to_all x2 -> x0, starting transfers between devices: 15.3 us -> none  [the longest x1 10.1 us: local(): lax.all_to_all(head_out, 'tp', split_axis=0, concat_axis=1, tiled=True)]
  transfers between devices with their start and end apart: 4 -> 0, of which waited for: 4 -> 0; matrix products, arithmetic and copies ran while one was open for 9% -> 0% of each run, Pallas kernels for 0% -> 0%
where the time goes in v1:
time: 260 us; the launch traced here: 258 us
  Pallas kernels  191 us (73%)
  matrix products  43.9 us (17%)
  other arithmetic  13.4 us (5%)
  local copies, waits for them, and re-layouts  9.04 us (3%)
    pallas_call x6, Pallas kernels, exchange(): pl.pallas_call(kernel, out_shape=jax.ShapeDtypeStruct(shape, block.dtype)...  191 us
    reduce_sum x2, other arithmetic, step(): new_total = run_total * factor + jnp.sum(expo_terms, axis=1)  7.89 us
    dot_general x2, matrix products, step(): lax.dot_general(query_rows, key_slab[:, :HEAD_SIZE], (((1,), (1,)), ((),...  7.53 us
    dot_general x2, matrix products, mix(): lax.dot_general(weights, returned, (((0,), (0,)), ((), ())), preferred_el...  7.37 us
    dot_general x1, matrix products, local(): jnp.dot(expert_inner, down_local, preferred_element_type=jnp.float32)  7.23 us
    dot_general x1, matrix products, local(): jnp.dot(shared_inner, shared_down, preferred_element_type=jnp.float32)  5.58 us

profile of v1, /device:TPU:13, one launch (start us, length us, event | category | flops | bytes accessed | tf_op | source)
XLA Modules:
  0.0 257.7 jit_solution(16841751889094646221)
XLA Ops:
  0.1 0.2 fusion.52
  0.3 1.1 copy.46
  1.5 0.7 mul.266
  2.2 0.1 multiply_multiply_fusion
  2.4 0.2 copy.52
  2.7 0.1 fusion.48
  2.8 0.2 subtract_convert_fusion.1
  3.0 0.1 copy.44
  3.2 0.1 copy.45
  3.3 0.7 pad_maximum_fusion.1.in_ref
  4.0 18.9 %exchange_0.1 = bf16[8,320,128]{2,1,0:T(8,128)(2,1)} custom-call(bf16[320,128]{1,0:T(8,128)(2,1)} %pad_maximum_fusion.1.in_ref), custom_call_target="tpu_custom_call" | custom-call | tf_op jit(solution)/shard_map/exchange_0/pallas_call | solution.py:84
  23.0 21.4 %while.15 = (s32[]{:T(128)}, f32[1280]{0:T(1024)S(1)}, f32[1280]{0:T(1024)S(1)}, f32[1280,64]{0,1:T(8,128)S(1)}, bf16[2,1280,128]{2,1,0:T(8,128)(2,1)}, /*index=5*/bf16[1280,64]{1,0:T(8,128)(2,1)S(1)}, s32[]{:T(128)}, s32[]{:T(128)}) while((s32[]{:T(128)}, f32[1280]{0:T(1024)S(1)}, f32[1280]{0:T(1024)S(1)}, ...), condition=%wide.region_5.6_spmd.clone, body=%wide.region_2.5_spmd.clone.sunk | while | flops 429512960 | bytes 48087168 | solution.py:184
  23.0 1.0 dynamic-slice_bitcast_fusion.2
  24.0 3.8 %fusion.95 = (f32[1280]{0:T(1024)S(1)}, f32[1280,1280]{1,0:T(8,128)}) fusion(bf16[1280,64]{1,0:T(8,128)(2,1)S(1)} %get-tuple-element.171, bf16[1280,128]{1,0:T(8,128)(2,1)S(1)} %dynamic-slice_bitcast_fusion.2), kind=kOutput, calls=%fused_computation.115.clone.1 | convolution fusion | flops 212990720 | bytes 7050240 | tf_op jit(solution)/shard_map/while/body/eval_jaxpr/dot_general | solution.py:165
  27.7 3.9 %fusion.96 = f32[1280]{0:T(1024)S(1)} fusion(f32[1280,1280]{1,0:T(8,128)} %get-tuple-element.147, f32[1280]{0:T(1024)S(1)} %select_maximum_fusion.2), kind=kLoop, calls=%fused_computation.3.clone.1 | loop fusion | flops 3275520 | bytes 6563840 | tf_op jit(solution)/shard_map/while/body/eval_jaxpr/reduce_sum | solution.py:176
  31.7 0.8 copy-done.1
  32.5 1.2 fusion.98
  33.7 1.0 dynamic-slice_bitcast_fusion.2
  34.7 3.8 %fusion.95 = (f32[1280]{0:T(1024)S(1)}, f32[1280,1280]{1,0:T(8,128)}) fusion(bf16[1280,64]{1,0:T(8,128)(2,1)S(1)} %get-tuple-element.171, bf16[1280,128]{1,0:T(8,128)(2,1)S(1)} %dynamic-slice_bitcast_fusion.2), kind=kOutput, calls=%fused_computation.115.clone.1 | convolution fusion | flops 212990720 | bytes 7050240 | tf_op jit(solution)/shard_map/while/body/eval_jaxpr/dot_general | solution.py:165
  38.5 3.9 %fusion.96 = f32[1280]{0:T(1024)S(1)} fusion(f32[1280,1280]{1,0:T(8,128)} %get-tuple-element.147, f32[1280]{0:T(1024)S(1)} %select_maximum_fusion.2), kind=kLoop, calls=%fused_computation.3.clone.1 | loop fusion | flops 3275520 | bytes 6563840 | tf_op jit(solution)/shard_map/while/body/eval_jaxpr/reduce_sum | solution.py:176
  42.4 0.8 copy-done.1
  43.2 1.2 fusion.98
  44.4 0.3 reshape.451
  44.8 0.1 mul.278
  44.9 0.1 fusion.41
  45.0 0.2 reshape_reshape.8
  45.2 0.8 copy.50.in_ref
  46.0 6.9 %exchange_1.1 = bf16[4,80,256]{2,1,0:T(8,128)(2,1)} custom-call(bf16[4,80,256]{2,1,0:T(8,128)(2,1)} %copy.50.in_ref), custom_call_target="tpu_custom_call" | custom-call | tf_op jit(solution)/shard_map/exchange_1/pallas_call | solution.py:84
  52.9 0.9 copy.54
  53.9 3.2 %multiply_reduce_fusion = (f32[80]{0:T(128)S(1)}, f32[80,2048]{1,0:T(8,128)S(1)}) fusion(bf16[80,1024]{1,0:T(8,128)(2,1)S(1)} %bitcast.94, bf16[1024,2048]{1,0:T(8,128)(2,1)} %param.25, bf16[320,2048]{1,0:T(8,128)(2,1)} %param.26, s32[]{:T(128)S(6)} %select_n.39), kind=kOutput, calls=%fused_computation.44 | convolution fusion | flops 336527296 | bytes 5341508 | tf_op jit(solution)/shard_map/dot_general | solution.py:199
  57.1 0.8 copy-done.4
  57.9 0.8 multiply_convert_fusion.in_ref
  58.8 18.8 %exchange_2.1 = bf16[4,80,2048]{2,1,0:T(8,128)(2,1)} custom-call(bf16[80,2048]{1,0:T(8,128)(2,1)} %multiply_convert_fusion.in_ref), custom_call_target="tpu_custom_call" | custom-call | tf_op jit(solution)/shard_map/exchange_2/pallas_call | solution.py:84
  77.6 0.1 compare_reduce_fusion
  77.7 0.1 fusion.27
  77.8 0.2 iota_compare_fusion
  78.1 4.4 %convolution_convert_fusion.1 = bf16[640,2048]{1,0:T(8,128)(2,1)} fusion(pred[640,320]{1,0:T(8,128)(4,1)S(1)} %bitcast.97, bf16[320,2048]{1,0:T(8,128)(2,1)} %bitcast.83), kind=kOutput, calls=%fused_computation.16 | convolution fusion | flops 840171520 | bytes 4136960 | tf_op jit(solution)/shard_map/dot_general | solution.py:220
  82.4 63.3 %exchange_3.1 = bf16[8,80,2048]{2,1,0:T(8,128)(2,1)} custom-call(bf16[8,80,2048]{2,1,0:T(8,128)(2,1)} %bitcast.91), custom_call_target="tpu_custom_call" | custom-call | tf_op jit(solution)/shard_map/exchange_3/pallas_call | solution.py:84
  145.7 5.0 %fusion.18 = f32[640,512]{1,0:T(8,128)} fusion(bf16[640,2048]{1,0:T(8,128)(2,1)} %bitcast.88, bf16[1,2048,512]{2,1,0:T(8,128)(2,1)} %param.30), kind=kOutput, calls=%fused_computation.29 | convolution fusion | flops 1342177280 | bytes 6029312 | tf_op jit(solution)/shard_map/dot_general | solution.py:226
  150.7 7.2 %convolution_convert_fusion = bf16[640,2048]{1,0:T(8,128)(2,1)} fusion(bf16[1,512,2048]{2,1,0:T(8,128)(2,1)S(1)} %copy-done, bf16[640,2048]{1,0:T(8,128)(2,1)} %bitcast.89, bf16[1,2048,512]{2,1,0:T(8,128)(2,1)} %param.31, f32[640,512]{1,0:T(8,128)} %fusion.18), kind=kOutput, calls=%fused_computation.15 | convolution fusion | flops 2687631360 | bytes 10747904 | tf_op jit(solution)/shard_map/dot_general | solution.py:229
  157.9 63.5 %exchange_4.1 = bf16[8,80,2048]{2,1,0:T(8,128)(2,1)} custom-call(bf16[8,80,2048]{2,1,0:T(8,128)(2,1)} %bitcast.90), custom_call_target="tpu_custom_call" | custom-call | tf_op jit(solution)/shard_map/exchange_4/pallas_call | solution.py:84
  221.5 4.6 %convolution_bitcast_fusion.1 = f32[320,2048]{1,0:T(8,128)} fusion(bf16[8,80,2048]{2,1,0:T(8,128)(2,1)} %exchange_4.1, f32[8,320]{1,0:T(8,128)S(1)} %bitcast.101, s32[8,320]{1,0:T(8,128)S(1)} %fusion.27), kind=kOutput, calls=%fused_computation.18 | convolution fusion | flops 839680000 | bytes 5263360 | tf_op jit(solution)/shard_map/dot_general | solution.py:241
  226.1 2.8 %convolution_bitcast_fusion = f32[320,2048]{1,0:T(8,128)} fusion(bf16[8,80,2048]{2,1,0:T(8,128)(2,1)S(1)} %copy-done.2, f32[8,320]{1,0:T(8,128)S(1)} %bitcast.102, s32[8,320]{1,0:T(8,128)S(1)} %fusion.27), kind=kOutput, calls=%fused_computation.17 | convolution fusion | flops 839884800 | bytes 5263360 | tf_op jit(solution)/shard_map/dot_general | solution.py:241
  228.9 1.2 fusion.69
  230.1 5.6 %fusion.12 = bf16[320,2048]{1,0:T(8,128)(2,1)} fusion(f32[320,2048]{1,0:T(8,128)} %convolution_bitcast_fusion, f32[320,2048]{1,0:T(8,128)} %convolution_bitcast_fusion.1, bf16[128,2048]{1,0:T(8,128)(2,1)} %param.35, bf16[320,2048]{1,0:T(8,128)(2,1)S(1)} %bitcast.85, bf16[2048,128]{1,0:T(8,128)(2,1)} %param.34, f32[320,128]{1,0:T(8,128)} %fusion.69), kind=kOutput, calls=%fused_computation.21 | convolution fusion | flops 337756160 | bytes 9076736 | tf_op jit(solution)/shard_map/dot_general | solution.py:249
  235.7 19.6 %exchange_5.1 = bf16[4,80,2048]{2,1,0:T(8,128)(2,1)} custom-call(bf16[4,80,2048]{2,1,0:T(8,128)(2,1)} %bitcast.87), custom_call_target="tpu_custom_call" | custom-call | tf_op jit(solution)/shard_map/exchange_5/pallas_call | solution.py:84
  255.2 1.6 convert_reduce_fusion
  256.9 0.8 add_convert_fusion
  (52 shorter events, 0.6 us)
Async XLA Ops:
  0.0 150.7 %copy-start = (bf16[1,512,2048]{2,1,0:T(8,128)(2,1)S(1)}, bf16[1,512,2048]{2,1,0:T(8,128)(2,1)}, u32[]{:S(2)}) copy-start(bf16[1,512,2048]{2,1,0:T(8,128)(2,1)} %param.32) | copy-start | bytes 6291460
  0.0 2.7 %copy-start.7 = (bf16[320,64]{0,1:T(8,128)(2,1)S(1)}, bf16[320,64]{0,1:T(8,128)(2,1)}, u32[]{:S(2)}) copy-start(bf16[320,64]{0,1:T(8,128)(2,1)} %param.20) | copy-start | bytes 122884
  0.0 2.7 %copy-start.13 = (f32[64]{0:T(128)S(1)}, f32[64]{0:T(128)}, u32[]{:S(2)}) copy-start(f32[64]{0:T(128)} %param.23) | copy-start | bytes 772
  0.0 3.1 %copy-start.8 = (bf16[320,64]{0,1:T(8,128)(2,1)S(1)}, bf16[320,64]{0,1:T(8,128)(2,1)}, u32[]{:S(2)}) copy-start(bf16[320,64]{0,1:T(8,128)(2,1)} %param.21) | copy-start | bytes 122884
  22.9 21.8 %copy-start.12 = (f32[256]{0:T(256)S(1)}, f32[256]{0:T(256)}, u32[]{:S(2)}) copy-start(f32[256]{0:T(256)} %param.24) | copy-start | bytes 3076
  27.7 4.7 %copy-start.1 = (f32[1280,1280]{1,0:T(8,128)S(1)}, f32[1280,1280]{1,0:T(8,128)}, u32[]{:S(2)}) copy-start(f32[1280,1280]{1,0:T(8,128)} %get-tuple-element.147) | copy-start | bytes 19660804 | tf_op jit(solution)/shard_map/while
  38.5 4.7 %copy-start.1 = (f32[1280,1280]{1,0:T(8,128)S(1)}, f32[1280,1280]{1,0:T(8,128)}, u32[]{:S(2)}) copy-start(f32[1280,1280]{1,0:T(8,128)} %get-tuple-element.147) | copy-start | bytes 19660804 | tf_op jit(solution)/shard_map/while
  53.9 4.1 %copy-start.10 = (f32[2048]{0:T(1024)S(1)}, f32[2048]{0:T(1024)}, u32[]{:S(2)}) copy-start(f32[2048]{0:T(1024)} %param.27) | copy-start | bytes 24580
  57.1 0.9 copy-start.4
  57.1 20.5 %copy-start.9 = (s32[320,4]{0,1:T(4,128)S(1)}, s32[320,4]{0,1:T(4,128)}, u32[]{:S(2)}) copy-start(s32[320,4]{0,1:T(4,128)} %param.28) | copy-start | bytes 15364
  157.9 63.5 %copy-start.11 = (f32[320,4]{0,1:T(4,128)S(1)}, f32[320,4]{0,1:T(4,128)}, u32[]{:S(2)}) copy-start(f32[320,4]{0,1:T(4,128)} %param.29) | copy-start | bytes 15364
  221.5 4.6 %copy-start.2 = (bf16[8,80,2048]{2,1,0:T(8,128)(2,1)S(1)}, bf16[8,80,2048]{2,1,0:T(8,128)(2,1)}, u32[]{:S(2)}) copy-start(bf16[8,80,2048]{2,1,0:T(8,128)(2,1)} %exchange_4.1) | copy-start | bytes 7864324
  226.1 2.8 %copy-start.3 = (bf16[4,80,2048]{2,1,0:T(8,128)(2,1)S(1)}, bf16[4,80,2048]{2,1,0:T(8,128)(2,1)}, u32[]{:S(2)}) copy-start(bf16[4,80,2048]{2,1,0:T(8,128)(2,1)} %exchange_2.1) | copy-start | bytes 3932164
  226.1 2.8 %copy-start.6 = (bf16[2048,128]{1,0:T(8,128)(2,1)S(1)}, bf16[2048,128]{1,0:T(8,128)(2,1)}, u32[]{:S(2)}) copy-start(bf16[2048,128]{1,0:T(8,128)(2,1)} %param.33) | copy-start | bytes 1572868
  235.7 21.2 %copy-start.5 = (f32[80,2048]{1,0:T(8,128)S(1)}, f32[80,2048]{1,0:T(8,128)}, u32[]{:S(2)}) copy-start(f32[80,2048]{1,0:T(8,128)} %copy-done.4) | copy-start | bytes 1966084

commit v2 on v1

--- a/solution.py
+++ b/solution.py
@@ -98,6 +98,377 @@
 
 def key_block_rows(piece_rows):
     return max((width for width in range(1, 2049) if piece_rows % width == 0))
+
+
+MESH = pl.DeviceIdType.MESH
+COLUMNS = 512
+
+
+def proxy_plane(t):
+    pair, side = t // 2, t % 2
+    return pair + side * (3 - 2 * pair)
+
+
+def proxy_of(plane):
+    return jnp.where(plane == 0, 0, jnp.where(plane == 3, 1, plane + 1))
+
+
+def place(planes, width, tp_count):
+    sp, t = lax.axis_index("sp"), lax.axis_index("tp")
+    z, x = sp // width, sp % width
+    return z, x, t, x * tp_count + t
+
+
+def greet(z, x, p, planes, width, tp_count):
+    barrier = pltpu.get_barrier_semaphore()
+    group = width * tp_count
+    for step in range(1, group):
+        peer = lax.rem(p + step, group)
+        pl.semaphore_signal(
+            barrier,
+            inc=1,
+            device_id={"sp": z * width + peer // tp_count, "tp": peer % tp_count},
+            device_id_type=MESH,
+        )
+    for step in (1, planes - 1):
+        pl.semaphore_signal(
+            barrier,
+            inc=1,
+            device_id={"sp": lax.rem(z + step, planes) * width + x},
+            device_id_type=MESH,
+        )
+    pl.semaphore_wait(barrier, group - 1 + 2)
+
+
+def dispatch(normed_own, select, planes, width, tp_count, call_id):
+    rows, model = normed_own.shape
+    group, capacity, tokens = select.shape
+    quarters = tokens // rows
+
+    def kernel(own_ref, sel_ref, out_ref, blk, packed, a_send, z_send, b_recv, c_send, c_recv, sem):
+        z, x, t, p = place(planes, width, tp_count)
+        zb = proxy_plane(t)
+        home = z == zb
+        greet(z, x, p, planes, width, tp_count)
+        target = proxy_of(z)
+
+        def to_home():
+            return pltpu.make_async_remote_copy(
+                src_ref=own_ref,
+                dst_ref=blk.at[t],
+                send_sem=a_send,
+                recv_sem=b_recv.at[t],
+                device_id={"tp": target},
+                device_id_type=MESH,
+            )
+
+        @pl.when(t != target)
+        def _():
+            to_home().start()
+
+        own_copy = pltpu.make_async_copy(own_ref, blk.at[t], sem)
+
+        @pl.when(home)
+        def _():
+            own_copy.start()
+            own_copy.wait()
+
+        def relay(q, up):
+            return pltpu.make_async_remote_copy(
+                src_ref=blk.at[q],
+                dst_ref=blk.at[q],
+                send_sem=z_send.at[up, q],
+                recv_sem=b_recv.at[q],
+                device_id={"sp": (z + (1 if up else -1)) * width + x},
+                device_id_type=MESH,
+            )
+
+        go_up = (z >= zb) & (z < planes - 1)
+        go_down = (z <= zb) & (z > 0)
+
+        for k in range(quarters):
+            q = lax.rem(t + k, quarters)
+
+            @pl.when(jnp.logical_not(home & (q == t)))
+            def _():
+                relay(q, 1).wait_recv()
+
+            @pl.when(go_up)
+            def _():
+                relay(q, 1).start()
+
+            @pl.when(go_down)
+            def _():
+                relay(q, 0).start()
+
+        def send(pp):
+            return pltpu.make_async_remote_copy(
+                src_ref=packed.at[pp],
+                dst_ref=out_ref.at[zb * width + x],
+                send_sem=c_send.at[pp],
+                recv_sem=c_recv.at[zb * width + x],
+                device_id={"sp": z * width + pp // tp_count, "tp": pp % tp_count},
+                device_id_type=MESH,
+            )
+
+        def serve(k, carry):
+            pp = lax.rem(p + 1 + k, group)
+            chosen = sel_ref[pp]
+            for column in range(0, model, COLUMNS):
+                part = pl.ds(column, COLUMNS)
+                packed[pp, :, part] = jnp.dot(
+                    chosen,
+                    blk[:, :, part].reshape(tokens, COLUMNS),
+                    preferred_element_type=jnp.float32,
+                ).astype(jnp.bfloat16)
+
+            @pl.when(pp != p)
+            def _():
+                send(pp).start()
+
+            return carry
+
+        lax.fori_loop(0, group, serve, 0)
+        kept = pltpu.make_async_copy(packed.at[p], out_ref.at[zb * width + x], sem)
+        kept.start()
+        kept.wait()
+
+        def finish(k, carry):
+            pp = lax.rem(p + 1 + k, group)
+            send(pp).wait_send()
+            source = proxy_plane(pp % tp_count) * width + pp // tp_count
+            pltpu.make_async_remote_copy(
+                src_ref=packed.at[pp],
+                dst_ref=out_ref.at[source],
+                send_sem=c_send.at[pp],
+                recv_sem=c_recv.at[source],
+                device_id={"sp": z * width + pp // tp_count, "tp": pp % tp_count},
+                device_id_type=MESH,
+            ).wait_recv()
+            return carry
+
+        lax.fori_loop(0, group - 1, finish, 0)
+
+        @pl.when(t != target)
+        def _():
+            to_home().wait_send()
+
+        for q in range(quarters):
+
+            @pl.when(go_up)
+            def _():
+                relay(q, 1).wait_send()
+
+            @pl.when(go_down)
+            def _():
+                relay(q, 0).wait_send()
+
+    vmem = pl.BlockSpec(memory_space=pltpu.VMEM)
+    dma = pltpu.SemaphoreType.DMA
+    return pl.pallas_call(
+        kernel,
+        out_shape=jax.ShapeDtypeStruct((planes * width, capacity, model), jnp.bfloat16),
+        in_specs=[vmem] * 2,
+        out_specs=vmem,
+        scratch_shapes=[
+            pltpu.VMEM((quarters, rows, model), jnp.bfloat16),
+            pltpu.VMEM((group, capacity, model), jnp.bfloat16),
+            dma,
+            dma((2, quarters)),
+            dma((quarters,)),
+            dma((group,)),
+            dma((planes * width,)),
+            dma,
+        ],
+        compiler_params=pltpu.CompilerParams(collective_id=call_id, has_side_effects=True),
+        name="dispatch",
+    )(normed_own, select)
+
+
+def give_back(produced, weights_hi, weights_lo, planes, width, tp_count, call_id):
+    blocks, capacity, model = produced.shape
+    quarters, rows, slots = weights_hi.shape
+    group = width * tp_count
+
+    def kernel(
+        in_ref, hi_ref, lo_ref, out_ref,
+        back, total, passed, arrived, c_send, c_recv, z_send, z_recv, a_recv, sem,
+    ):
+        z, x, t, p = place(planes, width, tp_count)
+        zb = proxy_plane(t)
+        home = z == zb
+        greet(z, x, p, planes, width, tp_count)
+        keep = pltpu.make_async_copy(in_ref.at[zb * width + x], back.at[p], sem)
+        keep.start()
+
+        def send(pp):
+            return pltpu.make_async_remote_copy(
+                src_ref=in_ref.at[proxy_plane(pp % tp_count) * width + pp // tp_count],
+                dst_ref=back.at[p],
+                send_sem=c_send.at[pp],
+                recv_sem=c_recv.at[p],
+                device_id={"sp": z * width + pp // tp_count, "tp": pp % tp_count},
+                device_id_type=MESH,
+            )
+
+        def came(pp):
+            return pltpu.make_async_remote_copy(
+                src_ref=in_ref.at[0],
+                dst_ref=back.at[pp],
+                send_sem=c_send.at[pp],
+                recv_sem=c_recv.at[pp],
+                device_id={"sp": z * width + pp // tp_count, "tp": pp % tp_count},
+                device_id_type=MESH,
+            )
+
+        def issue(k, carry):
+            rank = k // width
+            plane = jnp.where(2 * z < planes, planes - 1 - rank, rank)
+            pp = lax.rem(x + k + 1, width) * tp_count + proxy_of(plane)
+
+            @pl.when(pp != p)
+            def _():
+                send(pp).start()
+
+            return carry
+
+        lax.fori_loop(0, group, issue, 0)
+        keep.wait()
+
+        def collect(k, carry):
+            came(lax.rem(p + 1 + k, group)).wait_recv()
+            return carry
+
+        lax.fori_loop(0, group - 1, collect, 0)
+
+        from_above = (z >= zb) & (z < planes - 1)
+        from_below = (z <= zb) & (z > 0)
+
+        def hop(q, down):
+            return pltpu.make_async_remote_copy(
+                src_ref=passed.at[q],
+                dst_ref=arrived.at[down, q],
+                send_sem=z_send.at[q],
+                recv_sem=z_recv.at[down, q],
+                device_id={"sp": (z + (-1 if down else 1)) * width + x},
+                device_id_type=MESH,
+            )
+
+        def to_owner(q):
+            return pltpu.make_async_remote_copy(
+                src_ref=passed.at[q],
+                dst_ref=out_ref,
+                send_sem=z_send.at[q],
+                recv_sem=a_recv,
+                device_id={"tp": q},
+                device_id_type=MESH,
+            )
+
+        def quarter(q, carry):
+            for column in range(0, model, COLUMNS):
+                part = pl.ds(column, COLUMNS)
+                piece = back[:, :, part].reshape(slots, COLUMNS)
+                total[:, part] = jnp.dot(
+                    hi_ref[q], piece, preferred_element_type=jnp.float32
+                ) + jnp.dot(lo_ref[q], piece, preferred_element_type=jnp.float32)
+
+            @pl.when(from_above)
+            def _():
+                hop(q, 1).wait_recv()
+                total[...] += arrived[1, q].astype(jnp.float32)
+
+            @pl.when(from_below)
+            def _():
+                hop(q, 0).wait_recv()
+                total[...] += arrived[0, q].astype(jnp.float32)
+
+            passed[q] = total[...].astype(jnp.bfloat16)
+
+            @pl.when(z > zb)
+            def _():
+                hop(q, 1).start()
+
+            @pl.when(z < zb)
+            def _():
+                hop(q, 0).start()
+
+            @pl.when(home & (q != t))
+            def _():
+                to_owner(q).start()
+
+            @pl.when(home & (q == t))
+            def _():
+                mine = pltpu.make_async_copy(passed.at[q], out_ref, sem)
+                mine.start()
+                mine.wait()
+
+            return carry
+
+        lax.fori_loop(0, quarters, quarter, 0)
+
+        @pl.when(jnp.logical_not(home))
+        def _():
+            to_owner(t).wait_recv()
+
+        def sent(k, carry):
+            send(lax.rem(p + 1 + k, group)).wait_send()
+            return carry
+
+        lax.fori_loop(0, group - 1, sent, 0)
+
+        def left(q, carry):
+            @pl.when(jnp.logical_not(home & (q == t)))
+            def _():
+                to_owner(q).wait_send()
+
+            return carry
+
+        lax.fori_loop(0, quarters, left, 0)
+
+    vmem = pl.BlockSpec(memory_space=pltpu.VMEM)
+    dma = pltpu.SemaphoreType.DMA
+    return pl.pallas_call(
+        kernel,
+        out_shape=jax.ShapeDtypeStruct((rows, model), jnp.bfloat16),
+        in_specs=[vmem] * 3,
+        out_specs=vmem,
+        scratch_shapes=[
+            pltpu.VMEM((group, capacity, model), jnp.bfloat16),
+            pltpu.VMEM((rows, model), jnp.float32),
+            pltpu.VMEM((quarters, rows, model), jnp.bfloat16),
+            pltpu.VMEM((2, quarters, rows, model), jnp.bfloat16),
+            dma((group,)),
+            dma((group,)),
+            dma((quarters,)),
+            dma((2, quarters)),
+            dma,
+            dma,
+        ],
+        compiler_params=pltpu.CompilerParams(collective_id=call_id, has_side_effects=True),
+        name="give_back",
+    )(produced, weights_hi, weights_lo)
+
+
+def spread_shards(shard, tp_count):
+    across = lax.ppermute(shard, "tp", [(i, i ^ 2) for i in range(tp_count)])
+    beside = [(i, i ^ 1) for i in range(tp_count)]
+    return [shard, across, lax.ppermute(shard, "tp", beside), lax.ppermute(across, "tp", beside)]
+
+
+def slot_ranks(member):
+    order = jnp.arange(member.shape[0], dtype=jnp.int32)
+    before = (order[:, None] > order[None, :]).astype(jnp.bfloat16)
+    rank = jnp.dot(before, member.astype(jnp.bfloat16), preferred_element_type=jnp.float32)
+    return jnp.where(member, rank.astype(jnp.int32), -1)
+
+
+def expert_block(flat_rows, gate_local, up_local, down_local):
+    gate_out = jnp.dot(flat_rows, gate_local, preferred_element_type=jnp.float32)
+    up_out = jnp.dot(flat_rows, up_local, preferred_element_type=jnp.float32)
+    expert_inner = (jax.nn.silu(gate_out) * up_out).astype(jnp.bfloat16)
+    return jnp.dot(expert_inner, down_local, preferred_element_type=jnp.float32).astype(
+        jnp.bfloat16
+    )
 
 
 def local(
@@ -154,7 +525,29 @@
         jnp.zeros((head_count * tok_count, HEAD_SIZE), jnp.float32),
     )
     state = start_state
-    piece = exchange(packed, "sp", 0, True).reshape(sequence_total, 2 * HEAD_SIZE)
+    topk_count = routes.shape[1]
+    capacity = max(2, 2 * tok_count * topk_count // (sp_count * tp_count))
+    lanes = 2 * HEAD_SIZE
+    entries = tok_count * topk_count
+    relayed = (
+        tp_count == 4
+        and sp_count == 2 * tp_count
+        and capacity % 16 == 0
+        and tok_count % (16 * tp_count) == 0
+        and entries % lanes == 0
+    )
+    if relayed:
+        shared_shards = [spread_shards(w, tp_count) for w in (shared_gate, shared_up, shared_down)]
+        scale_hi = lax.reduce_precision(route_weights, 8, 7)
+        tables = jnp.stack([routes.astype(jnp.float32), scale_hi, route_weights - scale_hi])
+        tables = tables.astype(jnp.bfloat16).reshape(-1, lanes)
+        table_rows = tables.shape[0]
+        tables = jnp.pad(tables, ((0, -table_rows % 16), (0, 0)))
+        everything = exchange(jnp.concatenate([packed, tables], axis=0), "sp", 0, True)
+        piece = everything[:, :tok_count].reshape(sequence_total, lanes)
+        tables = everything[:, tok_count : tok_count + table_rows]
+    else:
+        piece = exchange(packed, "sp", 0, True).reshape(sequence_total, lanes)
     piece_rows = piece.shape[0]
     block_length = key_block_rows(piece_rows)
     key_blocks = piece.reshape(piece_rows // block_length, block_length, 2 * HEAD_SIZE)
@@ -200,34 +593,70 @@
     ).astype(jnp.bfloat16)
     normed_own = final_norm(hidden_own.astype(jnp.float32), ffn_gain).astype(jnp.bfloat16)
     model_width = normed_own.shape[1]
+    gate_local = expert_gate[0]
+    up_local = expert_up[0]
+    down_local = expert_down[0]
+    if relayed:
+        width = sp_count // tp_count
+        sp_index = lax.axis_index("sp")
+        stood_for = proxy_plane(tp_index) * width + sp_index % width
+        block_tables = lax.dynamic_index_in_dim(tables, stood_for, 0, keepdims=False)
+        block_tables = block_tables.astype(jnp.float32).reshape(3, tok_count, topk_count)
+        group = width * tp_count
+        plane_experts = (sp_index // width) * group + jnp.arange(group, dtype=jnp.int32)
+        named = block_tables[0].astype(jnp.int32)[:, :, None] == plane_experts[None, None, :]
+        rank = slot_ranks(jnp.any(named, axis=1))
+        slots = jnp.arange(capacity, dtype=jnp.int32)
+        select = (rank.T[:, None, :] == slots[None, :, None]).astype(jnp.bfloat16)
+        chosen = rank[:, :, None] == slots[None, None, :]
+
+        def combine(part):
+            scale = jnp.sum(jnp.where(named, block_tables[part][:, :, None], 0.0), axis=1)
+            table = jnp.where(chosen, scale[:, :, None], 0.0).astype(jnp.bfloat16)
+            return table.reshape(tp_count, part_rows, group * capacity)
+
+        combine_hi, combine_lo = combine(1), combine(2)
+        arrived = dispatch(normed_own, select, tp_count, width, tp_count, 2)
+        produced = expert_block(
+            arrived.reshape(sp_count * capacity, model_width), gate_local, up_local, down_local
+        )
+        gates, ups, downs = shared_shards
+        gate_part = jnp.dot(
+            normed_own, jnp.concatenate(gates, axis=1), preferred_element_type=jnp.float32
+        )
+        up_part = jnp.dot(
+            normed_own, jnp.concatenate(ups, axis=1), preferred_element_type=jnp.float32
+        )
+        shared_inner = (jax.nn.silu(gate_part) * up_part).astype(jnp.bfloat16)
+        shared_out = jnp.dot(
+            shared_inner, jnp.concatenate(downs, axis=0), preferred_element_type=jnp.float32
+        )
+        routed = give_back(
+            produced.reshape(sp_count, capacity, model_width),
+            combine_hi,
+            combine_lo,
+            tp_count,
+            width,
+            tp_count,
+            3,
+        )
+        return (
+            hidden_own.astype(jnp.float32) + (shared_out + routed.astype(jnp.float32))
+        ).astype(jnp.bfloat16)
     normed = exchange(normed_own, "tp", 2, True).reshape(tok_count, model_width)
-    topk_count = routes.shape[1]
-    capacity = max(2, 2 * tok_count * topk_count // (sp_count * tp_count))
     slot_total = sp_count * capacity
     experts_here = jnp.arange(sp_count, dtype=jnp.int32) * tp_count + tp_index
     named = routes[:, :, None] == experts_here[None, None, :]
     member = jnp.any(named, axis=1)
     scale = jnp.sum(jnp.where(named, route_weights[:, :, None], 0.0), axis=1)
-    order = jnp.arange(tok_count, dtype=jnp.int32)
-    before = (order[:, None] > order[None, :]).astype(jnp.bfloat16)
-    rank = jnp.dot(
-        before, member.astype(jnp.bfloat16), preferred_element_type=jnp.float32
-    ).astype(jnp.int32)
-    rank = jnp.where(member, rank, -1)
+    rank = slot_ranks(member)
     slots = jnp.arange(capacity, dtype=jnp.int32)
     chosen = rank.T[:, None, :] == slots[None, :, None]
     select = chosen.astype(jnp.bfloat16).reshape(slot_total, tok_count)
     outgoing = jnp.dot(select, normed, preferred_element_type=jnp.float32).astype(jnp.bfloat16)
-    gate_local = expert_gate[0]
-    up_local = expert_up[0]
-    down_local = expert_down[0]
     arrived = exchange(outgoing.reshape(sp_count, capacity, model_width), "sp", 3, False)
-    flat_rows = arrived.reshape(slot_total, model_width)
-    gate_out = jnp.dot(flat_rows, gate_local, preferred_element_type=jnp.float32)
-    up_out = jnp.dot(flat_rows, up_local, preferred_element_type=jnp.float32)
-    expert_inner = (jax.nn.silu(gate_out) * up_out).astype(jnp.bfloat16)
-    produced = jnp.dot(expert_inner, down_local, preferred_element_type=jnp.float32).astype(
-        jnp.bfloat16
+    produced = expert_block(
+        arrived.reshape(slot_total, model_width), gate_local, up_local, down_local
     )
     returned = exchange(produced.reshape(sp_count, capacity, model_width), "sp", 4, False).reshape(
         slot_total, model_width

time: 260 us -> 233 us (0.90)
  Pallas kernels: 191 us -> 157 us
  matrix products: 43.9 us -> 32.1 us
  local copies, waits for them, and re-layouts: 9.04 us -> 19.5 us
  other arithmetic: 13.4 us -> 18.7 us
  starting transfers between devices: 0 us -> 4.07 us
    pallas_call x6 -> x2, Pallas kernels: 191 us -> 27.2 us  [exchange(): pl.pallas_call(kernel, out_shape=jax.ShapeDtypeStruct(shape, block.dtype)...]
    pallas_call x0 -> x2, Pallas kernels: none -> 130 us  [the longest x1 72.3 us: give_back(): pl.pallas_call(kernel, out_shape=jax.ShapeDtypeStruct((rows, model), jnp....]
    dot_general x8 -> x5, matrix products: 30.9 us -> 19 us  [the longest x1 7.23 us: expert_block(): jnp.dot(expert_inner, down_local, preferred_element_type=jnp.float32)]
    broadcast_in_dim x0 -> x8, local copies, waits for them, and re-layouts: none -> 5.85 us  [the longest x4 5.32 us: combine(): table = jnp.where(chosen, scale[:, :, None], 0.0).astype(jnp.bfloat16)]
    ppermute x0 -> x9, starting transfers between devices: none -> 4.07 us  [the longest x3 1.76 us: spread_shards(): across = lax.ppermute(shard, 'tp', [(i, i ^ 2) for i in range(tp_count)])]
    convert_element_type x1 -> x4, other arithmetic: 0.81 us -> 4.87 us  [the longest x2 3.86 us: combine(): table = jnp.where(chosen, scale[:, :, None], 0.0).astype(jnp.bfloat16)]
    eq x0 -> x4, local copies, waits for them, and re-layouts: none -> 3.09 us  [local(): chosen = rank[:, :, None] == slots[None, None, :]]
  transfers between devices with their start and end apart: 0 -> 9, of which waited for: 0 -> 0; matrix products, arithmetic and copies ran while one was open for 0% -> 28% of each run, Pallas kernels for 0% -> 68%
where the time goes in v2:
time: 233 us; the launch traced here: 232 us
  Pallas kernels  157 us (67%)
  matrix products  32.1 us (14%)
  local copies, waits for them, and re-layouts  19.5 us (8%)
  other arithmetic  18.7 us (8%)
  starting transfers between devices  4.07 us (2%)
    pallas_call x1, Pallas kernels, give_back(): pl.pallas_call(kernel, out_shape=jax.ShapeDtypeStruct((rows, model), jnp....  72.3 us
    pallas_call x1, Pallas kernels, dispatch(): pl.pallas_call(kernel, out_shape=jax.ShapeDtypeStruct((planes * width, ca...  57.9 us
    pallas_call x2, Pallas kernels, exchange(): pl.pallas_call(kernel, out_shape=jax.ShapeDtypeStruct(shape, block.dtype)...  27.2 us
    reduce_sum x2, other arithmetic, step(): new_total = run_total * factor + jnp.sum(expo_terms, axis=1)  7.89 us
    dot_general x2, matrix products, step(): lax.dot_general(query_rows, key_slab[:, :HEAD_SIZE], (((1,), (1,)), ((),...  7.52 us
    dot_general x1, matrix products, expert_block(): jnp.dot(expert_inner, down_local, preferred_element_type=jnp.float32)  7.23 us
    broadcast_in_dim x4, local copies, waits for them, and re-layouts, combine(): table = jnp.where(chosen, scale[:, :, None], 0.0).astype(jnp.bfloat16)  5.32 us
    dot_general x1, matrix products, expert_block(): jnp.dot(flat_rows, gate_local, preferred_element_type=jnp.float32)  5 us
  transfers between devices with their start and end apart: 9, of which 0 were waited for; matrix products, arithmetic and copies ran while one was open for 28% of the time, Pallas kernels for 68%

profile of v2, /device:TPU:13, one launch (start us, length us, event | category | flops | bytes accessed | tf_op | source)
XLA Modules:
  0.0 232.3 jit_solution(7307887585469462048)
XLA Ops:
  0.0 0.3 collective-permute-start.6
  0.3 1.0 collective-permute-start.7
  1.3 1.2 collective-permute-start
  2.5 0.3 collective-permute-start.1
  2.8 0.2 collective-permute-start.3
  3.0 0.7 fusion.77
  3.7 0.7 fusion.75
  4.7 0.3 convert_element_type.112
  5.0 0.9 copy.45
  5.9 0.8 fusion.58
  6.8 0.9 fusion.59
  8.1 0.7 fusion.60.in_ref
  8.8 20.3 %exchange_0.1 = bf16[8,352,128]{2,1,0:T(8,128)(2,1)} custom-call(bf16[352,128]{1,0:T(8,128)(2,1)} %fusion.60.in_ref), custom_call_target="tpu_custom_call" | custom-call | tf_op jit(solution)/shard_map/exchange_0/pallas_call | solution.py:84
  29.1 2.0 slice.41
  32.0 21.4 %while.15 = (s32[]{:T(128)}, f32[1280]{0:T(1024)S(1)}, f32[1280]{0:T(1024)S(1)}, f32[1280,64]{0,1:T(8,128)S(1)}, bf16[2,1280,128]{2,1,0:T(8,128)(2,1)}, /*index=5*/bf16[1280,64]{1,0:T(8,128)(2,1)S(1)}, s32[]{:T(128)}, s32[]{:T(128)}) while((s32[]{:T(128)}, f32[1280]{0:T(1024)S(1)}, f32[1280]{0:T(1024)S(1)}, ...), condition=%wide.region_5.6_spmd.clone, body=%wide.region_2.5_spmd.clone.sunk | while | flops 429512960 | bytes 48087176 | solution.py:577
  32.1 1.0 dynamic-slice_bitcast_fusion.2
  33.1 3.8 %fusion.110 = (f32[1280]{0:T(1024)S(1)}, f32[1280,1280]{1,0:T(8,128)}) fusion(bf16[1280,64]{1,0:T(8,128)(2,1)S(1)} %get-tuple-element.180, bf16[1280,128]{1,0:T(8,128)(2,1)S(1)} %dynamic-slice_bitcast_fusion.2), kind=kOutput, calls=%fused_computation.136.clone.1 | convolution fusion | flops 212990720 | bytes 7050240 | tf_op jit(solution)/shard_map/while/body/eval_jaxpr/dot_general | solution.py:558
  36.8 3.9 %fusion.111 = f32[1280]{0:T(1024)S(1)} fusion(f32[1280,1280]{1,0:T(8,128)} %get-tuple-element.156, f32[1280]{0:T(1024)S(1)} %select_maximum_fusion.2), kind=kLoop, calls=%fused_computation.3.clone.1 | loop fusion | flops 3275520 | bytes 6563840 | tf_op jit(solution)/shard_map/while/body/eval_jaxpr/reduce_sum | solution.py:569
  40.8 0.8 copy-done.1
  41.6 1.2 fusion.113
  42.8 1.0 dynamic-slice_bitcast_fusion.2
  43.8 3.8 %fusion.110 = (f32[1280]{0:T(1024)S(1)}, f32[1280,1280]{1,0:T(8,128)}) fusion(bf16[1280,64]{1,0:T(8,128)(2,1)S(1)} %get-tuple-element.180, bf16[1280,128]{1,0:T(8,128)(2,1)S(1)} %dynamic-slice_bitcast_fusion.2), kind=kOutput, calls=%fused_computation.136.clone.1 | convolution fusion | flops 212990720 | bytes 7050240 | tf_op jit(solution)/shard_map/while/body/eval_jaxpr/dot_general | solution.py:558
  47.5 3.9 %fusion.111 = f32[1280]{0:T(1024)S(1)} fusion(f32[1280,1280]{1,0:T(8,128)} %get-tuple-element.156, f32[1280]{0:T(1024)S(1)} %select_maximum_fusion.2), kind=kLoop, calls=%fused_computation.3.clone.1 | loop fusion | flops 3275520 | bytes 6563840 | tf_op jit(solution)/shard_map/while/body/eval_jaxpr/reduce_sum | solution.py:569
  51.5 0.8 copy-done.1
  52.3 1.2 fusion.113
  53.5 0.3 reshape.425
  54.2 0.8 copy.51.in_ref
  55.1 7.0 %exchange_1.1 = bf16[4,80,256]{2,1,0:T(8,128)(2,1)} custom-call(bf16[4,80,256]{2,1,0:T(8,128)(2,1)} %copy.51.in_ref), custom_call_target="tpu_custom_call" | custom-call | tf_op jit(solution)/shard_map/exchange_1/pallas_call | solution.py:84
  62.0 0.9 copy.61
  63.0 3.2 %multiply_reduce_fusion = (f32[80]{0:T(128)S(1)}, f32[80,2048]{1,0:T(8,128)S(1)}) fusion(bf16[80,1024]{1,0:T(8,128)(2,1)S(1)} %bitcast.78, bf16[1024,2048]{1,0:T(8,128)(2,1)} %param.25, bf16[320,2048]{1,0:T(8,128)(2,1)} %param.26, s32[]{:T(128)S(6)} %select_n.68), kind=kOutput, calls=%fused_computation.60 | convolution fusion | flops 336527296 | bytes 5341508 | tf_op jit(solution)/shard_map/dot_general | solution.py:592
  66.8 1.0 fusion.50.sel_ref
  67.8 0.8 multiply_convert_fusion.own_ref
  68.7 57.9 %dispatch.1 = bf16[8,80,2048]{2,1,0:T(8,128)(2,1)} custom-call(bf16[80,2048]{1,0:T(8,128)(2,1)} %multiply_convert_fusion.own_ref, bf16[8,80,320]{2,1,0:T(8,128)(2,1)} %fusion.50.sel_ref), custom_call_target="tpu_custom_call" | custom-call | tf_op jit(solution)/shard_map/dispatch/pallas_call | solution.py:268
  126.6 5.0 %fusion.41 = f32[640,512]{1,0:T(8,128)} fusion(bf16[640,2048]{1,0:T(8,128)(2,1)} %bitcast.74, bf16[1,2048,512]{2,1,0:T(8,128)(2,1)} %param.30), kind=kOutput, calls=%fused_computation.48 | convolution fusion | flops 1342177280 | bytes 6029312 | tf_op jit(solution)/shard_map/dot_general | solution.py:466
  131.6 7.2 %convolution_convert_fusion = bf16[640,2048]{1,0:T(8,128)(2,1)} fusion(bf16[1,512,2048]{2,1,0:T(8,128)(2,1)S(1)} %copy-done, bf16[640,2048]{1,0:T(8,128)(2,1)} %bitcast.75, bf16[1,2048,512]{2,1,0:T(8,128)(2,1)} %param.31, f32[640,512]{1,0:T(8,128)} %fusion.41), kind=kOutput, calls=%fused_computation.15 | convolution fusion | flops 2687631360 | bytes 10747904 | tf_op jit(solution)/shard_map/dot_general | solution.py:469
  139.8 0.4 broadcast_in_dim.97
  140.3 1.3 broadcast_in_dim.98
  141.5 1.3 eq.58
  142.8 1.7 eq.59
  144.8 1.3 broadcast_in_dim.92
  146.0 2.4 %broadcast_in_dim.93 = bf16[4,80,640]{2,1,0:T(8,128)(2,1)} reshape(bf16[320,8,80]{2,1,0:T(8,128)(2,1)} %broadcast_in_dim.92) | data formatting | bytes 819200 | tf_op jit(solution)/shard_map/jit(_where)/broadcast_in_dim | solution.py:615
  148.4 2.0 select_convert_fusion
  150.4 0.5 collective-permute-start.4
  151.0 0.4 collective-permute-start.5
  151.4 1.9 select_convert_fusion.1.hi_ref
  153.3 72.3 %give_back.1 = bf16[80,2048]{1,0:T(8,128)(2,1)} custom-call(bf16[8,80,2048]{2,1,0:T(8,128)(2,1)} %bitcast.73, bf16[4,80,640]{2,1,0:T(8,128)(2,1)} %select_convert_fusion.1.hi_ref, bf16[4,80,640]{2,1,0:T(8,128)(2,1)} %get-tuple-element.89.lo_ref), custom_call_target="tpu_custom_call" | custom-call | tf_op jit(solution)/shard_map/give_back/pallas_call | solution.py:430
  225.6 2.7 %fusion.15 = f32[80,512]{1,0:T(8,128)} fusion(bf16[80,2048]{1,0:T(8,128)(2,1)S(1)} %copy-done.4, bf16[2048,128]{1,0:T(8,128)(2,1)} %collective-permute-done.2, bf16[2048,128]{1,0:T(8,128)(2,1)} %collective-permute-done.1, bf16[2048,128]{1,0:T(8,128)(2,1)} %collective-permute-done, bf16[2048,128]{1,0:T(8,128)(2,1)} %param.33), kind=kOutput, calls=%fused_computation.22 | convolution fusion | flops 176160768 | bytes 2588672 | tf_op jit(solution)/shard_map/dot_general | solution.py:624
  228.4 3.9 %fusion.12 = bf16[80,2048]{1,0:T(8,128)(2,1)} fusion(f32[80,2048]{1,0:T(8,128)S(1)} %copy-done.3, bf16[128,2048]{1,0:T(8,128)(2,1)} %collective-permute-done.8, bf16[128,2048]{1,0:T(8,128)(2,1)} %collective-permute-done.7, bf16[128,2048]{1,0:T(8,128)(2,1)} %collective-permute-done.6, bf16[128,2048]{1,0:T(8,128)(2,1)} %param.35, ...), kind=kOutput, calls=%fused_computation.19 | convolution fusion | flops 353222656 | bytes 5996544 | tf_op jit(solution)/shard_map/dot_general | solution.py:631
  (84 shorter events, 3.9 us)
Async XLA Ops:
  0.0 131.6 %copy-start = (bf16[1,512,2048]{2,1,0:T(8,128)(2,1)S(1)}, bf16[1,512,2048]{2,1,0:T(8,128)(2,1)}, u32[]{:S(2)}) copy-start(bf16[1,512,2048]{2,1,0:T(8,128)(2,1)} %param.32) | copy-start | bytes 6291460
  0.0 31.1 %copy-start.9 = (f32[64]{0:T(128)S(1)}, f32[64]{0:T(128)}, u32[]{:S(2)}) copy-start(f32[64]{0:T(128)} %param.22) | copy-start | bytes 772
  0.0 31.2 %copy-start.6 = (bf16[320,256]{1,0:T(8,128)(2,1)S(1)}, bf16[320,256]{1,0:T(8,128)(2,1)}, u32[]{:S(2)}) copy-start(bf16[320,256]{1,0:T(8,128)(2,1)} %param.19) | copy-start | bytes 491524
  0.0 150.4 %collective-permute-start.6 = (bf16[128,2048]{1,0:T(8,128)(2,1)}, bf16[128,2048]{1,0:T(8,128)(2,1)}, u32[]{:S(2)}, u32[]{:S(2)}) collective-permute-start(bf16[128,2048]{1,0:T(8,128)(2,1)} %param.35), channel_id=1, source_target_pairs={{0,2},{1,3},{2,0},{3,1},{4,6},{5,7},{6,4},{7,5},{8,10},{9,11},{10,... | collective-permute-start | bytes 1572872 | tf_op jit(solution)/shard_map/ppermute | solution.py:453
  0.3 228.1 %collective-permute-start.7 = (bf16[128,2048]{1,0:T(8,128)(2,1)}, bf16[128,2048]{1,0:T(8,128)(2,1)}, u32[]{:S(2)}, u32[]{:S(2)}) collective-permute-start(bf16[128,2048]{1,0:T(8,128)(2,1)} %param.35), channel_id=1, source_target_pairs={{0,1},{1,0},{2,3},{3,2},{4,5},{5,4},{6,7},{7,6},{8,9},{9,8},{10,11... | collective-permute-start | bytes 1572872 | tf_op jit(solution)/shard_map/ppermute | solution.py:455
  1.3 138.2 %collective-permute-start = (bf16[2048,128]{1,0:T(8,128)(2,1)}, bf16[2048,128]{1,0:T(8,128)(2,1)}, u32[]{:S(2)}, u32[]{:S(2)}) collective-permute-start(bf16[2048,128]{1,0:T(8,128)(2,1)} %param.33), channel_id=1, source_target_pairs={{0,2},{1,3},{2,0},{3,1},{4,6},{5,7},{6,4},{7,5},{8,10},{9,11},{10,... | collective-permute-start | bytes 1572872 | tf_op jit(solution)/shard_map/ppermute | solution.py:453
  2.5 148.4 %collective-permute-start.1 = (bf16[2048,128]{1,0:T(8,128)(2,1)}, bf16[2048,128]{1,0:T(8,128)(2,1)}, u32[]{:S(2)}, u32[]{:S(2)}) collective-permute-start(bf16[2048,128]{1,0:T(8,128)(2,1)} %param.33), channel_id=1, source_target_pairs={{0,1},{1,0},{2,3},{3,2},{4,5},{5,4},{6,7},{7,6},{8,9},{9,8},{10,11... | collective-permute-start | bytes 1572872 | tf_op jit(solution)/shard_map/ppermute | solution.py:455
  2.8 148.2 %collective-permute-start.3 = (bf16[2048,128]{1,0:T(8,128)(2,1)}, bf16[2048,128]{1,0:T(8,128)(2,1)}, u32[]{:S(2)}, u32[]{:S(2)}) collective-permute-start(bf16[2048,128]{1,0:T(8,128)(2,1)} %param.34), channel_id=1, source_target_pairs={{0,2},{1,3},{2,0},{3,1},{4,6},{5,7},{6,4},{7,5},{8,10},{9,11},{10,... | collective-permute-start | bytes 1572872 | tf_op jit(solution)/shard_map/ppermute | solution.py:453
  32.0 21.8 %copy-start.8 = (f32[256]{0:T(256)S(1)}, f32[256]{0:T(256)}, u32[]{:S(2)}) copy-start(f32[256]{0:T(256)} %param.24) | copy-start | bytes 3076
  36.8 4.7 %copy-start.1 = (f32[1280,1280]{1,0:T(8,128)S(1)}, f32[1280,1280]{1,0:T(8,128)}, u32[]{:S(2)}) copy-start(f32[1280,1280]{1,0:T(8,128)} %get-tuple-element.156) | copy-start | bytes 19660804 | tf_op jit(solution)/shard_map/while
  47.5 4.7 %copy-start.1 = (f32[1280,1280]{1,0:T(8,128)S(1)}, f32[1280,1280]{1,0:T(8,128)}, u32[]{:S(2)}) copy-start(f32[1280,1280]{1,0:T(8,128)} %get-tuple-element.156) | copy-start | bytes 19660804 | tf_op jit(solution)/shard_map/while
  63.0 3.3 %slice-start = ((bf16[8,352,128]{2,1,0:T(8,128)(2,1)}), bf16[8,30,128]{2,1,0:T(8,128)(2,1)S(1)}, s32[]{:S(2)}) async-start(bf16[8,352,128]{2,1,0:T(8,128)(2,1)} %exchange_0.1), calls=%async_computation | async-start | bytes 131072 | tf_op jit(solution)/shard_map/slice | solution.py:548
  63.0 4.9 %copy-start.7 = (f32[2048]{0:T(1024)S(1)}, f32[2048]{0:T(1024)}, u32[]{:S(2)}) copy-start(f32[2048]{0:T(1024)} %param.27) | copy-start | bytes 24580
  66.3 60.4 %copy-start.2 = (f32[80,2048]{1,0:T(8,128)}, f32[80,2048]{1,0:T(8,128)S(1)}, u32[]{:S(2)}) copy-start(f32[80,2048]{1,0:T(8,128)S(1)} %get-tuple-element.111) | copy-start | bytes 1966084
  139.4 86.2 %collective-permute-start.2 = (bf16[2048,128]{1,0:T(8,128)(2,1)}, bf16[2048,128]{1,0:T(8,128)(2,1)}, u32[]{:S(2)}, u32[]{:S(2)}) collective-permute-start(bf16[2048,128]{1,0:T(8,128)(2,1)} %collective-permute-done), channel_id=1, source_target_pairs={{0,1},{1,0},{2,3},{3,2},{4,5},{5,4},{6,7},{7,6},{8,9},{9,8},{10,11... | collective-permute-start | bytes 1572872 | tf_op jit(solution)/shard_map/ppermute | solution.py:455
  150.4 75.2 %copy-start.4 = (bf16[80,2048]{1,0:T(8,128)(2,1)S(1)}, bf16[80,2048]{1,0:T(8,128)(2,1)}, u32[]{:S(2)}) copy-start(bf16[80,2048]{1,0:T(8,128)(2,1)} %multiply_convert_fusion.own_ref) | copy-start | bytes 983044
  150.4 78.0 %collective-permute-start.4 = (bf16[2048,128]{1,0:T(8,128)(2,1)}, bf16[2048,128]{1,0:T(8,128)(2,1)}, u32[]{:S(2)}, u32[]{:S(2)}) collective-permute-start(bf16[2048,128]{1,0:T(8,128)(2,1)} %param.34), channel_id=1, source_target_pairs={{0,1},{1,0},{2,3},{3,2},{4,5},{5,4},{6,7},{7,6},{8,9},{9,8},{10,11... | collective-permute-start | bytes 1572872 | tf_op jit(solution)/shard_map/ppermute | solution.py:455
  150.9 77.5 %collective-permute-start.8 = (bf16[128,2048]{1,0:T(8,128)(2,1)}, bf16[128,2048]{1,0:T(8,128)(2,1)}, u32[]{:S(2)}, u32[]{:S(2)}) collective-permute-start(bf16[128,2048]{1,0:T(8,128)(2,1)} %collective-permute-done.6), channel_id=1, source_target_pairs={{0,1},{1,0},{2,3},{3,2},{4,5},{5,4},{6,7},{7,6},{8,9},{9,8},{10,11... | collective-permute-start | bytes 1572872 | tf_op jit(solution)/shard_map/ppermute | solution.py:455
  151.0 77.4 %collective-permute-start.5 = (bf16[2048,128]{1,0:T(8,128)(2,1)}, bf16[2048,128]{1,0:T(8,128)(2,1)}, u32[]{:S(2)}, u32[]{:S(2)}) collective-permute-start(bf16[2048,128]{1,0:T(8,128)(2,1)} %collective-permute-done.3), channel_id=1, source_target_pairs={{0,1},{1,0},{2,3},{3,2},{4,5},{5,4},{6,7},{7,6},{8,9},{9,8},{10,11... | collective-permute-start | bytes 1572872 | tf_op jit(solution)/shard_map/ppermute | solution.py:455
  225.6 2.8 %copy-start.3 = (f32[80,2048]{1,0:T(8,128)S(1)}, f32[80,2048]{1,0:T(8,128)}, u32[]{:S(2)}) copy-start(f32[80,2048]{1,0:T(8,128)} %copy-done.2) | copy-start | bytes 1966084
  225.6 2.8 %copy-start.5 = (bf16[80,2048]{1,0:T(8,128)(2,1)S(1)}, bf16[80,2048]{1,0:T(8,128)(2,1)}, u32[]{:S(2)}) copy-start(bf16[80,2048]{1,0:T(8,128)(2,1)} %give_back.1) | copy-start | bytes 983044

commit v3 on v2

--- a/solution.py
+++ b/solution.py
@@ -287,12 +287,13 @@
 
 def give_back(produced, weights_hi, weights_lo, planes, width, tp_count, call_id):
     blocks, capacity, model = produced.shape
-    quarters, rows, slots = weights_hi.shape
-    group = width * tp_count
+    group, quarters = width * tp_count, tp_count
+    slots, tokens = weights_hi.shape
+    rows = tokens // quarters
 
     def kernel(
         in_ref, hi_ref, lo_ref, out_ref,
-        back, total, passed, arrived, c_send, c_recv, z_send, z_recv, a_recv, sem,
+        back, high, low, total, passed, arrived, c_send, c_recv, z_send, z_recv, a_recv, sem,
     ):
         z, x, t, p = place(planes, width, tp_count)
         zb = proxy_plane(t)
@@ -333,6 +334,8 @@
             return carry
 
         lax.fori_loop(0, group, issue, 0)
+        high[...] = hi_ref[...].T.reshape(quarters, rows, slots)
+        low[...] = lo_ref[...].T.reshape(quarters, rows, slots)
         keep.wait()
 
         def collect(k, carry):
@@ -369,8 +372,8 @@
                 part = pl.ds(column, COLUMNS)
                 piece = back[:, :, part].reshape(slots, COLUMNS)
                 total[:, part] = jnp.dot(
-                    hi_ref[q], piece, preferred_element_type=jnp.float32
-                ) + jnp.dot(lo_ref[q], piece, preferred_element_type=jnp.float32)
+                    high[q], piece, preferred_element_type=jnp.float32
+                ) + jnp.dot(low[q], piece, preferred_element_type=jnp.float32)
 
             @pl.when(from_above)
             def _():
@@ -434,6 +437,8 @@
         out_specs=vmem,
         scratch_shapes=[
             pltpu.VMEM((group, capacity, model), jnp.bfloat16),
+            pltpu.VMEM((quarters, rows, slots), jnp.bfloat16),
+            pltpu.VMEM((quarters, rows, slots), jnp.bfloat16),
             pltpu.VMEM((rows, model), jnp.float32),
             pltpu.VMEM((quarters, rows, model), jnp.bfloat16),
             pltpu.VMEM((2, quarters, rows, model), jnp.bfloat16),
@@ -447,6 +452,159 @@
         compiler_params=pltpu.CompilerParams(collective_id=call_id, has_side_effects=True),
         name="give_back",
     )(produced, weights_hi, weights_lo)
+
+
+def attend(queries_t, own, gain, tokens, width, call_id):
+    count = lax.axis_size("sp")
+    planes = count // width
+    span = queries_t.shape[1]
+    heads = gain.shape[0]
+    chunk = 256
+
+    def kernel(q_ref, own_ref, gain_ref, all_ref, out_ref, top, norm, acc, z_send, x_send, recv, sem):
+        me = lax.axis_index("sp")
+        z, x = me // width, me % width
+        beside = z * width + (1 - x)
+        barrier = pltpu.get_barrier_semaphore()
+        peers = [lax.rem(z + step, planes) * width + x for step in range(1, planes)] + [beside]
+        for peer in peers:
+            pl.semaphore_signal(barrier, inc=1, device_id={"sp": peer}, device_id_type=MESH)
+        kept = pltpu.make_async_copy(own_ref, all_ref.at[me], sem)
+        kept.start()
+        pl.semaphore_wait(barrier, len(peers))
+
+        def along(step):
+            return pltpu.make_async_remote_copy(
+                src_ref=own_ref,
+                dst_ref=all_ref.at[me],
+                send_sem=z_send.at[step],
+                recv_sem=recv.at[me],
+                device_id={"sp": lax.rem(z + step, planes) * width + x},
+                device_id_type=MESH,
+            )
+
+        def across(step, column):
+            source = lax.rem(z + step, planes) * width + column
+            return pltpu.make_async_remote_copy(
+                src_ref=own_ref if step == 0 else all_ref.at[source],
+                dst_ref=all_ref.at[source],
+                send_sem=x_send.at[step],
+                recv_sem=recv.at[source],
+                device_id={"sp": beside},
+                device_id_type=MESH,
+            )
+
+        across(0, x).start()
+        for step in range(1, planes):
+            along(step).start()
+        kept.wait()
+
+        def absorb(slot, first):
+            keys = all_ref[slot, 0:tokens, 0:HEAD_SIZE]
+            vals = all_ref[slot, 0:tokens, HEAD_SIZE : 2 * HEAD_SIZE]
+            for start in range(0, span, chunk):
+                part = pl.ds(start, chunk)
+                scores = jnp.dot(keys, q_ref[:, part], preferred_element_type=jnp.float32)
+                peak = jnp.max(scores, axis=0, keepdims=True)
+                if not first:
+                    old = top[:, part]
+                    peak = jnp.maximum(old, peak)
+                    factor = jnp.exp(old - peak)
+                terms = jnp.exp(scores - peak)
+                amount = jnp.sum(terms, axis=0, keepdims=True)
+                mixed = lax.dot_general(
+                    vals,
+                    terms.astype(jnp.bfloat16),
+                    (((0,), (0,)), ((), ())),
+                    preferred_element_type=jnp.float32,
+                )
+                if not first:
+                    amount = norm[:, part] * factor + amount
+                    mixed = acc[:, part] * factor + mixed
+                top[:, part] = peak
+                norm[:, part] = amount
+                acc[:, part] = mixed
+
+        def block(step, column):
+            return lax.rem(z + step, planes) * width + column
+
+        absorb(me, True)
+        for step in range(1, planes + 1):
+            if step < planes:
+                across(step, x).wait_recv()
+                across(step, x).start()
+            across(step - 1, 1 - x).wait_recv()
+            absorb(block(step - 1, 1 - x), False)
+            if step < planes:
+                absorb(block(step, x), False)
+
+        attended = acc[...] / norm[...]
+        mean_sq = jnp.mean(attended * attended, axis=0, keepdims=True)
+        rows = (attended * lax.rsqrt(mean_sq + EPS)).T
+        for h in range(heads):
+            out_ref[:, h * HEAD_SIZE : (h + 1) * HEAD_SIZE] = (
+                rows[h * tokens : (h + 1) * tokens] * gain_ref[h : h + 1, :]
+            ).astype(jnp.bfloat16)
+        for step in range(planes):
+            if step > 0:
+                along(step).wait_send()
+            across(step, x).wait_send()
+
+    vmem = pl.BlockSpec(memory_space=pltpu.VMEM)
+    dma = pltpu.SemaphoreType.DMA
+    return pl.pallas_call(
+        kernel,
+        out_shape=(
+            jax.ShapeDtypeStruct((count,) + own.shape, jnp.bfloat16),
+            jax.ShapeDtypeStruct((tokens, heads * HEAD_SIZE), jnp.bfloat16),
+        ),
+        in_specs=[vmem] * 3,
+        out_specs=(vmem, vmem),
+        scratch_shapes=[
+            pltpu.VMEM((1, span), jnp.float32),
+            pltpu.VMEM((1, span), jnp.float32),
+            pltpu.VMEM((HEAD_SIZE, span), jnp.float32),
+            dma((planes,)),
+            dma((planes,)),
+            dma((count,)),
+            dma,
+        ],
+        compiler_params=pltpu.CompilerParams(collective_id=call_id, has_side_effects=True),
+        name="attend",
+    )(queries_t, own, gain)
+
+
+def scan_attention(query_rows, key_blocks, score_scale):
+    start_state = (
+        jnp.full((query_rows.shape[0],), -1e30, jnp.float32),
+        jnp.zeros((query_rows.shape[0],), jnp.float32),
+        jnp.zeros(query_rows.shape, jnp.float32),
+    )
+
+    def step(carry, key_slab):
+        run_max, run_total, run_acc = carry
+        scores = (
+            lax.dot_general(
+                query_rows,
+                key_slab[:, :HEAD_SIZE],
+                (((1,), (1,)), ((), ())),
+                preferred_element_type=jnp.float32,
+            )
+            * score_scale
+        )
+        new_max = jnp.maximum(run_max, jnp.max(scores, axis=1))
+        factor = jnp.exp(run_max - new_max)
+        expo_terms = jnp.exp(scores - new_max[:, None])
+        new_total = run_total * factor + jnp.sum(expo_terms, axis=1)
+        new_acc = run_acc * factor[:, None] + jnp.dot(
+            expo_terms.astype(jnp.bfloat16),
+            key_slab[:, HEAD_SIZE:],
+            preferred_element_type=jnp.float32,
+        )
+        return ((new_max, new_total, new_acc), None)
+
+    (_, run_total, run_acc), _ = lax.scan(step, start_state, key_blocks)
+    return run_acc / run_total[:, None]
 
 
 def spread_shards(shard, tp_count):
@@ -517,14 +675,7 @@
         .astype(jnp.bfloat16)
     )
     packed = jnp.concatenate([rotated_key, values], axis=1)
-    query_rows = rotated_query.transpose(1, 0, 2).reshape(head_count * tok_count, HEAD_SIZE)
     score_scale = HEAD_SIZE ** (-0.5)
-    start_state = (
-        jnp.full((head_count * tok_count,), -1e30, jnp.float32),
-        jnp.zeros((head_count * tok_count,), jnp.float32),
-        jnp.zeros((head_count * tok_count, HEAD_SIZE), jnp.float32),
-    )
-    state = start_state
     topk_count = routes.shape[1]
     capacity = max(2, 2 * tok_count * topk_count // (sp_count * tp_count))
     lanes = 2 * HEAD_SIZE
@@ -535,6 +686,7 @@
         and capacity % 16 == 0
         and tok_count % (16 * tp_count) == 0
         and entries % lanes == 0
+        and head_count * tok_count % 256 == 0
     )
     if relayed:
         shared_shards = [spread_shards(w, tp_count) for w in (shared_gate, shared_up, shared_down)]
@@ -543,44 +695,25 @@
         tables = tables.astype(jnp.bfloat16).reshape(-1, lanes)
         table_rows = tables.shape[0]
         tables = jnp.pad(tables, ((0, -table_rows % 16), (0, 0)))
-        everything = exchange(jnp.concatenate([packed, tables], axis=0), "sp", 0, True)
-        piece = everything[:, :tok_count].reshape(sequence_total, lanes)
+        scaled = rotated_query * jnp.asarray(score_scale, jnp.bfloat16)
+        everything, head_out = attend(
+            scaled.transpose(2, 1, 0).reshape(HEAD_SIZE, head_count * tok_count),
+            jnp.concatenate([packed, tables], axis=0),
+            head_gain.reshape(head_count, HEAD_SIZE),
+            tok_count,
+            sp_count // tp_count,
+            0,
+        )
         tables = everything[:, tok_count : tok_count + table_rows]
     else:
         piece = exchange(packed, "sp", 0, True).reshape(sequence_total, lanes)
-    piece_rows = piece.shape[0]
-    block_length = key_block_rows(piece_rows)
-    key_blocks = piece.reshape(piece_rows // block_length, block_length, 2 * HEAD_SIZE)
-
-    def step(carry, key_slab):
-        run_max, run_total, run_acc = carry
-        scores = (
-            lax.dot_general(
-                query_rows,
-                key_slab[:, :HEAD_SIZE],
-                (((1,), (1,)), ((), ())),
-                preferred_element_type=jnp.float32,
-            )
-            * score_scale
-        )
-        new_max = jnp.maximum(run_max, jnp.max(scores, axis=1))
-        factor = jnp.exp(run_max - new_max)
-        expo_terms = jnp.exp(scores - new_max[:, None])
-        new_total = run_total * factor + jnp.sum(expo_terms, axis=1)
-        new_acc = run_acc * factor[:, None] + jnp.dot(
-            expo_terms.astype(jnp.bfloat16),
-            key_slab[:, HEAD_SIZE:],
-            preferred_element_type=jnp.float32,
-        )
-        return ((new_max, new_total, new_acc), None)
-
-    state, _ = lax.scan(step, state, key_blocks)
-    run_max, run_total, run_acc = state
-    attended = (
-        (run_acc / run_total[:, None]).reshape(head_count, tok_count, HEAD_SIZE).transpose(1, 0, 2)
-    )
-    head_out = final_norm(attended, head_gain.reshape(head_count, HEAD_SIZE)).astype(jnp.bfloat16)
-    head_out = head_out.reshape(tok_count, head_count * HEAD_SIZE)
+        query_rows = rotated_query.transpose(1, 0, 2).reshape(head_count * tok_count, HEAD_SIZE)
+        block_length = key_block_rows(sequence_total)
+        key_blocks = piece.reshape(sequence_total // block_length, block_length, lanes)
+        attended = scan_attention(query_rows, key_blocks, score_scale)
+        attended = attended.reshape(head_count, tok_count, HEAD_SIZE).transpose(1, 0, 2)
+        head_out = final_norm(attended, head_gain.reshape(head_count, HEAD_SIZE))
+        head_out = head_out.astype(jnp.bfloat16).reshape(tok_count, head_count * HEAD_SIZE)
     part_rows = tok_count // tp_count
     token_heads = exchange(
         head_out.reshape(tp_count, part_rows, head_count * HEAD_SIZE), "tp", 1, False
@@ -608,12 +741,11 @@
         rank = slot_ranks(jnp.any(named, axis=1))
         slots = jnp.arange(capacity, dtype=jnp.int32)
         select = (rank.T[:, None, :] == slots[None, :, None]).astype(jnp.bfloat16)
-        chosen = rank[:, :, None] == slots[None, None, :]
 
         def combine(part):
             scale = jnp.sum(jnp.where(named, block_tables[part][:, :, None], 0.0), axis=1)
-            table = jnp.where(chosen, scale[:, :, None], 0.0).astype(jnp.bfloat16)
-            return table.reshape(tp_count, part_rows, group * capacity)
+            table = select * scale.T.astype(jnp.bfloat16)[:, None, :]
+            return table.reshape(group * capacity, tok_count)
 
         combine_hi, combine_lo = combine(1), combine(2)
         arrived = dispatch(normed_own, select, tp_count, width, tp_count, 2)

time: 233 us -> 199 us (0.85)
  other arithmetic: 18.7 us -> 4.83 us
  local copies, waits for them, and re-layouts: 19.5 us -> 6.93 us
  matrix products: 32.1 us -> 22.2 us
  Pallas kernels: 157 us -> 161 us
    pallas_call x0 -> x1, Pallas kernels: none -> 25.5 us  [attend(): pl.pallas_call(kernel, out_shape=(jax.ShapeDtypeStruct((count,) + own.sha...]
    pallas_call x2 -> x1, Pallas kernels: 27.2 us -> 6.65 us  [exchange(): pl.pallas_call(kernel, out_shape=jax.ShapeDtypeStruct(shape, block.dtype)...]
    dot_general x4 -> x0, matrix products: 9.88 us -> none  [the longest x2 7.52 us: step(): lax.dot_general(query_rows, key_slab[:, :HEAD_SIZE], (((1,), (1,)), ((),...]
    reduce_sum x2 -> x0, other arithmetic: 7.89 us -> none  [step(): new_total = run_total * factor + jnp.sum(expo_terms, axis=1)]
    broadcast_in_dim x4 -> x0, local copies, waits for them, and re-layouts: 5.32 us -> none  [combine(): table = jnp.where(chosen, scale[:, :, None], 0.0).astype(jnp.bfloat16)]
    convert_element_type x3 -> x0, other arithmetic: 3.97 us -> none  [the longest x2 3.86 us: combine(): table = jnp.where(chosen, scale[:, :, None], 0.0).astype(jnp.bfloat16)]
    eq x4 -> x2, local copies, waits for them, and re-layouts: 3.09 us -> 0.1 us  [local(): select = (rank.T[:, None, :] == slots[None, :, None]).astype(jnp.bfloat16)]
    pallas_call x1, Pallas kernels: 57.9 us -> 55.6 us  [dispatch(): pl.pallas_call(kernel, out_shape=jax.ShapeDtypeStruct((planes * width, ca...]
  transfers between devices with their start and end apart: 9 -> 9, of which waited for: 0 -> 0; matrix products, arithmetic and copies ran while one was open for 28% -> 15% of each run, Pallas kernels for 68% -> 81%
where the time goes in v3:
time: 199 us
  Pallas kernels  161 us (81%)
  matrix products  22.2 us (11%)
  local copies, waits for them, and re-layouts  6.93 us (3%)
  other arithmetic  4.83 us (2%)
  starting transfers between devices  4.01 us (2%)
    pallas_call x1, Pallas kernels, give_back(): pl.pallas_call(kernel, out_shape=jax.ShapeDtypeStruct((rows, model), jnp....  73 us
    pallas_call x1, Pallas kernels, dispatch(): pl.pallas_call(kernel, out_shape=jax.ShapeDtypeStruct((planes * width, ca...  55.6 us
    pallas_call x1, Pallas kernels, attend(): pl.pallas_call(kernel, out_shape=(jax.ShapeDtypeStruct((count,) + own.sha...  25.5 us
    dot_general x1, matrix products, expert_block(): jnp.dot(expert_inner, down_local, preferred_element_type=jnp.float32)  7.22 us
    pallas_call x1, Pallas kernels, exchange(): pl.pallas_call(kernel, out_shape=jax.ShapeDtypeStruct(shape, block.dtype)...  6.65 us
    dot_general x1, matrix products, expert_block(): jnp.dot(flat_rows, gate_local, preferred_element_type=jnp.float32)  5.01 us
  transfers between devices with their start and end apart: 9, of which 0 were waited for; matrix products, arithmetic and copies ran while one was open for 15% of the time, Pallas kernels for 81%

profile of v3, /device:TPU:13, one launch (start us, length us, event | category | flops | bytes accessed | tf_op | source)
XLA Modules:
  0.0 199.0 jit_solution(846728766358458997)
XLA Ops:
  0.0 0.3 collective-permute-start
  0.3 1.0 collective-permute-start.1
  1.3 1.2 collective-permute-start.3
  2.5 0.3 collective-permute-start.4
  2.8 0.2 collective-permute-start.6
  3.1 1.1 copy.30
  4.2 0.1 bitcast_reduce_fusion
  4.2 0.7 mul.249
  5.0 0.1 fusion.60
  5.1 0.2 fusion.59
  5.3 0.1 multiply_multiply_fusion
  5.5 0.2 copy.41
  5.6 0.8 reshape.415.q_ref
  6.5 0.1 fusion.47
  6.6 0.2 subtract_convert_fusion.1
  6.8 0.1 copy.32
  7.0 0.2 copy.34
  7.2 0.3 convert_element_type.107
  7.6 0.1 copy.33
  7.7 0.6 reshape.417.gain_ref
  8.3 0.7 fusion.48.own_ref
  9.1 25.5 %attend.1 = (bf16[8,352,128]{2,1,0:T(8,128)(2,1)}, bf16[320,256]{1,0:T(8,128)(2,1)}) custom-call(bf16[64,1280]{1,0:T(8,128)(2,1)} %reshape.415.q_ref, bf16[352,128]{1,0:T(8,128)(2,1)} %fusion.48.own_ref, f32[4,64]{1,0:T(4,128)} %reshape.417.gain_ref), custom_call_target="tpu_custom_call" | custom-call | tf_op jit(solution)/shard_map/attend/pallas_call | solution.py:555
  34.6 0.8 slice.34
  35.5 0.2 convert_element_type.114
  35.6 0.1 copy.36
  35.7 0.1 compare_reduce_fusion
  35.8 0.1 fusion.38
  36.0 6.7 %exchange_1.1 = bf16[4,80,256]{2,1,0:T(8,128)(2,1)} custom-call(bf16[4,80,256]{2,1,0:T(8,128)(2,1)} %bitcast.80), custom_call_target="tpu_custom_call" | custom-call | tf_op jit(solution)/shard_map/exchange_1/pallas_call | solution.py:84
  42.6 0.9 copy.39
  43.6 3.2 %multiply_reduce_fusion = (f32[80]{0:T(128)S(1)}, f32[80,2048]{1,0:T(8,128)S(1)}) fusion(bf16[80,1024]{1,0:T(8,128)(2,1)S(1)} %bitcast.74, bf16[1024,2048]{1,0:T(8,128)(2,1)} %param.23, bf16[320,2048]{1,0:T(8,128)(2,1)} %param.24, s32[]{:T(128)S(6)} %select_n.56), kind=kOutput, calls=%fused_computation.46 | convolution fusion | flops 336527296 | bytes 5341508 | tf_op jit(solution)/shard_map/dot_general | solution.py:725
  46.8 0.9 multiply_convert_fusion.own_ref
  47.7 0.9 fusion.41.sel_ref
  48.6 55.6 %dispatch.1 = bf16[8,80,2048]{2,1,0:T(8,128)(2,1)} custom-call(bf16[80,2048]{1,0:T(8,128)(2,1)} %multiply_convert_fusion.own_ref, bf16[8,80,320]{2,1,0:T(8,128)(2,1)} %fusion.41.sel_ref), custom_call_target="tpu_custom_call" | custom-call | tf_op jit(solution)/shard_map/dispatch/pallas_call | solution.py:268
  104.1 5.0 %fusion.30 = f32[640,512]{1,0:T(8,128)} fusion(bf16[640,2048]{1,0:T(8,128)(2,1)} %bitcast.68, bf16[1,2048,512]{2,1,0:T(8,128)(2,1)} %param.28), kind=kOutput, calls=%fused_computation.33 | convolution fusion | flops 1342177280 | bytes 6029312 | tf_op jit(solution)/shard_map/dot_general | solution.py:624
  109.2 0.5 collective-permute-start.2
  109.7 0.1 collective-permute-start.5
  109.7 0.4 collective-permute-start.8
  110.2 7.2 %convolution_convert_fusion = bf16[640,2048]{1,0:T(8,128)(2,1)} fusion(bf16[1,512,2048]{2,1,0:T(8,128)(2,1)S(1)} %copy-done, bf16[640,2048]{1,0:T(8,128)(2,1)} %bitcast.69, bf16[1,2048,512]{2,1,0:T(8,128)(2,1)} %param.29, f32[640,512]{1,0:T(8,128)} %fusion.30), kind=kOutput, calls=%fused_computation | convolution fusion | flops 2687631360 | bytes 10747904 | tf_op jit(solution)/shard_map/dot_general | solution.py:627
  117.4 0.2 broadcast_in_dim.23
  117.6 0.1 copy.37
  117.7 0.2 broadcast_in_dim.30
  117.9 0.1 copy.38
  117.9 0.1 eq.51
  118.0 0.1 fusion.55
  118.1 1.2 fusion.39
  119.4 73.0 %give_back.1 = bf16[80,2048]{1,0:T(8,128)(2,1)} custom-call(bf16[8,80,2048]{2,1,0:T(8,128)(2,1)} %bitcast.70, bf16[640,320]{1,0:T(8,128)(2,1)} %get-tuple-element.18.hi_ref, bf16[640,320]{1,0:T(8,128)(2,1)} %get-tuple-element.17.lo_ref), custom_call_target="tpu_custom_call" | custom-call | tf_op jit(solution)/shard_map/give_back/pallas_call | solution.py:433
  192.4 2.7 %fusion.4 = f32[80,512]{1,0:T(8,128)} fusion(bf16[80,2048]{1,0:T(8,128)(2,1)S(1)} %copy-done.1, bf16[2048,128]{1,0:T(8,128)(2,1)} %collective-permute-done.2, bf16[2048,128]{1,0:T(8,128)(2,1)} %copy-done.10, bf16[2048,128]{1,0:T(8,128)(2,1)} %collective-permute-done, bf16[2048,128]{1,0:T(8,128)(2,1)} %param.31), kind=kOutput, calls=%fused_computation.7 | convolution fusion | flops 176160768 | bytes 2588672 | tf_op jit(solution)/shard_map/dot_general | solution.py:756
  195.1 3.9 %fusion.1 = bf16[80,2048]{1,0:T(8,128)(2,1)} fusion(f32[80,2048]{1,0:T(8,128)S(1)} %get-tuple-element.31, bf16[128,2048]{1,0:T(8,128)(2,1)} %collective-permute-done.8, bf16[128,2048]{1,0:T(8,128)(2,1)} %collective-permute-done.7, bf16[128,2048]{1,0:T(8,128)(2,1)} %collective-permute-done.6, bf16[128,2048]{1,0:T(8,128)(2,1)} %param.33, ...), kind=kOutput, calls=%fused_computation.4 | convolution fusion | flops 353222656 | bytes 5996544 | tf_op jit(solution)/shard_map/dot_general | solution.py:763
  (48 shorter events, 0.3 us)
Async XLA Ops:
  0.0 110.2 %copy-start = (bf16[1,512,2048]{2,1,0:T(8,128)(2,1)S(1)}, bf16[1,512,2048]{2,1,0:T(8,128)(2,1)}, u32[]{:S(2)}) copy-start(bf16[1,512,2048]{2,1,0:T(8,128)(2,1)} %param.30) | copy-start | bytes 6291460
  0.0 6.5 %copy-start.3 = (bf16[320,64]{0,1:T(8,128)(2,1)S(1)}, bf16[320,64]{0,1:T(8,128)(2,1)}, u32[]{:S(2)}) copy-start(bf16[320,64]{0,1:T(8,128)(2,1)} %param.18) | copy-start | bytes 122884
  0.0 6.5 %copy-start.9 = (f32[64]{0:T(128)S(1)}, f32[64]{0:T(128)}, u32[]{:S(2)}) copy-start(f32[64]{0:T(128)} %param.21) | copy-start | bytes 772
  0.0 6.9 %copy-start.6 = (f32[320,4]{0,1:T(4,128)S(1)}, f32[320,4]{0,1:T(4,128)}, u32[]{:S(2)}) copy-start(f32[320,4]{0,1:T(4,128)} %param.27) | copy-start | bytes 15364
  0.0 7.0 %copy-start.7 = (s32[320,4]{0,1:T(4,128)S(1)}, s32[320,4]{0,1:T(4,128)}, u32[]{:S(2)}) copy-start(s32[320,4]{0,1:T(4,128)} %param.26) | copy-start | bytes 15364
  0.0 109.1 %collective-permute-start = (bf16[2048,128]{1,0:T(8,128)(2,1)}, bf16[2048,128]{1,0:T(8,128)(2,1)}, u32[]{:S(2)}, u32[]{:S(2)}) collective-permute-start(bf16[2048,128]{1,0:T(8,128)(2,1)} %param.31), channel_id=1, source_target_pairs={{0,2},{1,3},{2,0},{3,1},{4,6},{5,7},{6,4},{7,5},{8,10},{9,11},{10,... | collective-permute-start | bytes 1572872 | tf_op jit(solution)/shard_map/ppermute | solution.py:611
  0.3 108.8 %collective-permute-start.1 = (bf16[2048,128]{1,0:T(8,128)(2,1)}, bf16[2048,128]{1,0:T(8,128)(2,1)S(1)}, u32[]{:S(2)}, u32[]{:S(2)}) collective-permute-start(bf16[2048,128]{1,0:T(8,128)(2,1)} %param.31), channel_id=1, source_target_pairs={{0,1},{1,0},{2,3},{3,2},{4,5},{5,4},{6,7},{7,6},{8,9},{9,8},{10,11... | collective-permute-start | bytes 1572872 | tf_op jit(solution)/shard_map/ppermute | solution.py:613
  1.3 108.4 %collective-permute-start.3 = (bf16[2048,128]{1,0:T(8,128)(2,1)}, bf16[2048,128]{1,0:T(8,128)(2,1)}, u32[]{:S(2)}, u32[]{:S(2)}) collective-permute-start(bf16[2048,128]{1,0:T(8,128)(2,1)} %param.32), channel_id=1, source_target_pairs={{0,2},{1,3},{2,0},{3,1},{4,6},{5,7},{6,4},{7,5},{8,10},{9,11},{10,... | collective-permute-start | bytes 1572872 | tf_op jit(solution)/shard_map/ppermute | solution.py:611
  2.5 192.6 %collective-permute-start.4 = (bf16[2048,128]{1,0:T(8,128)(2,1)}, bf16[2048,128]{1,0:T(8,128)(2,1)}, u32[]{:S(2)}, u32[]{:S(2)}) collective-permute-start(bf16[2048,128]{1,0:T(8,128)(2,1)} %param.32), channel_id=1, source_target_pairs={{0,1},{1,0},{2,3},{3,2},{4,5},{5,4},{6,7},{7,6},{8,9},{9,8},{10,11... | collective-permute-start | bytes 1572872 | tf_op jit(solution)/shard_map/ppermute | solution.py:613
  2.8 106.9 %collective-permute-start.6 = (bf16[128,2048]{1,0:T(8,128)(2,1)}, bf16[128,2048]{1,0:T(8,128)(2,1)}, u32[]{:S(2)}, u32[]{:S(2)}) collective-permute-start(bf16[128,2048]{1,0:T(8,128)(2,1)} %param.33), channel_id=1, source_target_pairs={{0,2},{1,3},{2,0},{3,1},{4,6},{5,7},{6,4},{7,5},{8,10},{9,11},{10,... | collective-permute-start | bytes 1572872 | tf_op jit(solution)/shard_map/ppermute | solution.py:611
  4.1 3.4 %copy-start.4 = (bf16[320,64]{0,1:T(8,128)(2,1)S(1)}, bf16[320,64]{0,1:T(8,128)(2,1)}, u32[]{:S(2)}) copy-start(bf16[320,64]{0,1:T(8,128)(2,1)} %param.19) | copy-start | bytes 122884
  4.2 3.5 %copy-start.8 = (f32[256]{0:T(256)S(1)}, f32[256]{0:T(256)}, u32[]{:S(2)}) copy-start(f32[256]{0:T(256)} %param.22) | copy-start | bytes 3076
  43.5 3.3 %copy-start.5 = (f32[2048]{0:T(1024)S(1)}, f32[2048]{0:T(1024)}, u32[]{:S(2)}) copy-start(f32[2048]{0:T(1024)} %param.25) | copy-start | bytes 24580
  109.1 86.0 %collective-permute-start.7 = (bf16[128,2048]{1,0:T(8,128)(2,1)}, bf16[128,2048]{1,0:T(8,128)(2,1)}, u32[]{:S(2)}, u32[]{:S(2)}) collective-permute-start(bf16[128,2048]{1,0:T(8,128)(2,1)} %param.33), channel_id=1, source_target_pairs={{0,1},{1,0},{2,3},{3,2},{4,5},{5,4},{6,7},{7,6},{8,9},{9,8},{10,11... | collective-permute-start | bytes 1572872 | tf_op jit(solution)/shard_map/ppermute | solution.py:613
  109.2 8.3 %copy-start.10 = (bf16[2048,128]{1,0:T(8,128)(2,1)}, bf16[2048,128]{1,0:T(8,128)(2,1)S(1)}, u32[]{:S(2)}) copy-start(bf16[2048,128]{1,0:T(8,128)(2,1)S(1)} %collective-permute-done.1) | copy-start | bytes 1572868
  109.2 83.2 %collective-permute-start.2 = (bf16[2048,128]{1,0:T(8,128)(2,1)}, bf16[2048,128]{1,0:T(8,128)(2,1)}, u32[]{:S(2)}, u32[]{:S(2)}) collective-permute-start(bf16[2048,128]{1,0:T(8,128)(2,1)} %collective-permute-done), channel_id=1, source_target_pairs={{0,1},{1,0},{2,3},{3,2},{4,5},{5,4},{6,7},{7,6},{8,9},{9,8},{10,11... | collective-permute-start | bytes 1572872 | tf_op jit(solution)/shard_map/ppermute | solution.py:613
  109.7 85.4 %collective-permute-start.5 = (bf16[2048,128]{1,0:T(8,128)(2,1)}, bf16[2048,128]{1,0:T(8,128)(2,1)}, u32[]{:S(2)}, u32[]{:S(2)}) collective-permute-start(bf16[2048,128]{1,0:T(8,128)(2,1)} %collective-permute-done.3), channel_id=1, source_target_pairs={{0,1},{1,0},{2,3},{3,2},{4,5},{5,4},{6,7},{7,6},{8,9},{9,8},{10,11... | collective-permute-start | bytes 1572872 | tf_op jit(solution)/shard_map/ppermute | solution.py:613
  109.7 85.4 %collective-permute-start.8 = (bf16[128,2048]{1,0:T(8,128)(2,1)}, bf16[128,2048]{1,0:T(8,128)(2,1)}, u32[]{:S(2)}, u32[]{:S(2)}) collective-permute-start(bf16[128,2048]{1,0:T(8,128)(2,1)} %collective-permute-done.6), channel_id=1, source_target_pairs={{0,1},{1,0},{2,3},{3,2},{4,5},{5,4},{6,7},{7,6},{8,9},{9,8},{10,11... | collective-permute-start | bytes 1572872 | tf_op jit(solution)/shard_map/ppermute | solution.py:613
  119.4 73.0 %copy-start.1 = (bf16[80,2048]{1,0:T(8,128)(2,1)S(1)}, bf16[80,2048]{1,0:T(8,128)(2,1)}, u32[]{:S(2)}) copy-start(bf16[80,2048]{1,0:T(8,128)(2,1)} %multiply_convert_fusion.own_ref) | copy-start | bytes 983044
  192.3 2.8 %copy-start.2 = (bf16[80,2048]{1,0:T(8,128)(2,1)S(1)}, bf16[80,2048]{1,0:T(8,128)(2,1)}, u32[]{:S(2)}) copy-start(bf16[80,2048]{1,0:T(8,128)(2,1)} %give_back.1) | copy-start | bytes 983044

commit v4 on v3

--- a/solution.py
+++ b/solution.py
@@ -140,12 +140,18 @@
     pl.semaphore_wait(barrier, group - 1 + 2)
 
 
-def dispatch(normed_own, select, planes, width, tp_count, call_id):
+def dispatch(normed_own, select, shards, planes, width, tp_count, call_id):
     rows, model = normed_own.shape
     group, capacity, tokens = select.shape
     quarters = tokens // rows
 
-    def kernel(own_ref, sel_ref, out_ref, blk, packed, a_send, z_send, b_recv, c_send, c_recv, sem):
+    given = len(shards)
+
+    def kernel(own_ref, sel_ref, *refs):
+        shard_refs, out_ref, pair_refs = refs[:given], refs[given], refs[given + 1 : 2 * given + 1]
+        blk, packed, a_send, z_send, b_recv, c_send, c_recv, w_send, w_recv, sem = refs[
+            2 * given + 1 :
+        ]
         z, x, t, p = place(planes, width, tp_count)
         zb = proxy_plane(t)
         home = z == zb
@@ -166,6 +172,19 @@
         def _():
             to_home().start()
 
+        pairs = [
+            pltpu.make_async_remote_copy(
+                src_ref=shard_refs[i],
+                dst_ref=pair_refs[i],
+                send_sem=w_send.at[i],
+                recv_sem=w_recv.at[i],
+                device_id={"tp": t + 1 - 2 * lax.rem(t, 2)},
+                device_id_type=MESH,
+            )
+            for i in range(given)
+        ]
+        for copy in pairs:
+            copy.start()
         own_copy = pltpu.make_async_copy(own_ref, blk.at[t], sem)
 
         @pl.when(home)
@@ -263,13 +282,17 @@
             def _():
                 relay(q, 0).wait_send()
 
+        for copy in pairs:
+            copy.wait()
+
     vmem = pl.BlockSpec(memory_space=pltpu.VMEM)
     dma = pltpu.SemaphoreType.DMA
     return pl.pallas_call(
         kernel,
-        out_shape=jax.ShapeDtypeStruct((planes * width, capacity, model), jnp.bfloat16),
-        in_specs=[vmem] * 2,
-        out_specs=vmem,
+        out_shape=[jax.ShapeDtypeStruct((planes * width, capacity, model), jnp.bfloat16)]
+        + [jax.ShapeDtypeStruct(w.shape, w.dtype) for w in shards],
+        in_specs=[vmem] * 2 + [pl.BlockSpec(memory_space=pl.ANY)] * given,
+        out_specs=[vmem] + [pl.BlockSpec(memory_space=pl.ANY)] * given,
         scratch_shapes=[
             pltpu.VMEM((quarters, rows, model), jnp.bfloat16),
             pltpu.VMEM((group, capacity, model), jnp.bfloat16),
@@ -278,23 +301,28 @@
             dma((quarters,)),
             dma((group,)),
             dma((planes * width,)),
+            dma((given,)),
+            dma((given,)),
             dma,
         ],
         compiler_params=pltpu.CompilerParams(collective_id=call_id, has_side_effects=True),
         name="dispatch",
-    )(normed_own, select)
-
-
-def give_back(produced, weights_hi, weights_lo, planes, width, tp_count, call_id):
+    )(normed_own, select, *shards)
+
+
+def give_back(produced, weights_hi, weights_lo, own, shards, planes, width, tp_count, call_id):
     blocks, capacity, model = produced.shape
     group, quarters = width * tp_count, tp_count
     slots, tokens = weights_hi.shape
     rows = tokens // quarters
 
-    def kernel(
-        in_ref, hi_ref, lo_ref, out_ref,
-        back, high, low, total, passed, arrived, c_send, c_recv, z_send, z_recv, a_recv, sem,
-    ):
+    pieces = len(shards) // 3
+
+    def kernel(in_ref, hi_ref, lo_ref, own_ref, *refs):
+        gates, ups = refs[:pieces], refs[pieces : 2 * pieces]
+        downs, refs = refs[2 * pieces : 3 * pieces], refs[3 * pieces :]
+        out_ref, shared_ref, back, high, low, total, passed, arrived = refs[:8]
+        c_send, c_recv, z_send, z_recv, a_recv, sem = refs[8:]
         z, x, t, p = place(planes, width, tp_count)
         zb = proxy_plane(t)
         home = z == zb
@@ -336,6 +364,17 @@
         lax.fori_loop(0, group, issue, 0)
         high[...] = hi_ref[...].T.reshape(quarters, rows, slots)
         low[...] = lo_ref[...].T.reshape(quarters, rows, slots)
+        for i in range(pieces):
+            gate = jnp.dot(own_ref[...], gates[i][...], preferred_element_type=jnp.float32)
+            up = jnp.dot(own_ref[...], ups[i][...], preferred_element_type=jnp.float32)
+            inner = (gate / (1.0 + jnp.exp(-gate)) * up).astype(jnp.bfloat16)
+            for column in range(0, model, COLUMNS):
+                part = pl.ds(column, COLUMNS)
+                share = jnp.dot(inner, downs[i][:, part], preferred_element_type=jnp.float32)
+                if i == 0:
+                    shared_ref[:, part] = share
+                else:
+                    shared_ref[:, part] += share
         keep.wait()
 
         def collect(k, carry):
@@ -432,9 +471,12 @@
     dma = pltpu.SemaphoreType.DMA
     return pl.pallas_call(
         kernel,
-        out_shape=jax.ShapeDtypeStruct((rows, model), jnp.bfloat16),
-        in_specs=[vmem] * 3,
-        out_specs=vmem,
+        out_shape=(
+            jax.ShapeDtypeStruct((rows, model), jnp.bfloat16),
+            jax.ShapeDtypeStruct((rows, model), jnp.float32),
+        ),
+        in_specs=[vmem] * (4 + 3 * pieces),
+        out_specs=(vmem, vmem),
         scratch_shapes=[
             pltpu.VMEM((group, capacity, model), jnp.bfloat16),
             pltpu.VMEM((quarters, rows, slots), jnp.bfloat16),
@@ -451,27 +493,40 @@
         ],
         compiler_params=pltpu.CompilerParams(collective_id=call_id, has_side_effects=True),
         name="give_back",
-    )(produced, weights_hi, weights_lo)
-
-
-def attend(queries_t, own, gain, tokens, width, call_id):
+    )(produced, weights_hi, weights_lo, own, *shards)
+
+
+def attend(queries_t, own, gain, tokens, width, tp_count, call_id):
     count = lax.axis_size("sp")
     planes = count // width
     span = queries_t.shape[1]
     heads = gain.shape[0]
     chunk = 256
 
-    def kernel(q_ref, own_ref, gain_ref, all_ref, out_ref, top, norm, acc, z_send, x_send, recv, sem):
-        me = lax.axis_index("sp")
+    rows_each = tokens // tp_count
+    features = heads * HEAD_SIZE
+
+    def kernel(
+        q_ref, own_ref, gain_ref, all_ref, heads_ref,
+        out_ref, top, norm, acc, z_send, x_send, recv, h_send, h_recv, sem,
+    ):
+        me, t = lax.axis_index("sp"), lax.axis_index("tp")
         z, x = me // width, me % width
         beside = z * width + (1 - x)
         barrier = pltpu.get_barrier_semaphore()
         peers = [lax.rem(z + step, planes) * width + x for step in range(1, planes)] + [beside]
         for peer in peers:
             pl.semaphore_signal(barrier, inc=1, device_id={"sp": peer}, device_id_type=MESH)
+        for step in range(1, tp_count):
+            pl.semaphore_signal(
+                barrier,
+                inc=1,
+                device_id={"tp": lax.rem(t + step, tp_count)},
+                device_id_type=MESH,
+            )
         kept = pltpu.make_async_copy(own_ref, all_ref.at[me], sem)
         kept.start()
-        pl.semaphore_wait(barrier, len(peers))
+        pl.semaphore_wait(barrier, len(peers) + tp_count - 1)
 
         def along(step):
             return pltpu.make_async_remote_copy(
@@ -545,6 +600,29 @@
             out_ref[:, h * HEAD_SIZE : (h + 1) * HEAD_SIZE] = (
                 rows[h * tokens : (h + 1) * tokens] * gain_ref[h : h + 1, :]
             ).astype(jnp.bfloat16)
+        mine = heads_ref.at[:, pl.ds(pl.multiple_of(t * features, 128), features)]
+
+        def part_of(peer):
+            return out_ref.at[pl.ds(pl.multiple_of(peer * rows_each, 16), rows_each)]
+
+        swaps = []
+        for step in range(1, tp_count):
+            peer = lax.rem(t + step, tp_count)
+            swap = pltpu.make_async_remote_copy(
+                src_ref=part_of(peer),
+                dst_ref=mine,
+                send_sem=h_send.at[step],
+                recv_sem=h_recv.at[step],
+                device_id={"tp": peer},
+                device_id_type=MESH,
+            )
+            swap.start()
+            swaps.append(swap)
+        kept = pltpu.make_async_copy(part_of(t), mine, sem)
+        kept.start()
+        kept.wait()
+        for swap in swaps:
+            swap.wait()
         for step in range(planes):
             if step > 0:
                 along(step).wait_send()
@@ -556,17 +634,20 @@
         kernel,
         out_shape=(
             jax.ShapeDtypeStruct((count,) + own.shape, jnp.bfloat16),
-            jax.ShapeDtypeStruct((tokens, heads * HEAD_SIZE), jnp.bfloat16),
+            jax.ShapeDtypeStruct((rows_each, tp_count * features), jnp.bfloat16),
         ),
         in_specs=[vmem] * 3,
         out_specs=(vmem, vmem),
         scratch_shapes=[
+            pltpu.VMEM((tokens, features), jnp.bfloat16),
             pltpu.VMEM((1, span), jnp.float32),
             pltpu.VMEM((1, span), jnp.float32),
             pltpu.VMEM((HEAD_SIZE, span), jnp.float32),
             dma((planes,)),
             dma((planes,)),
             dma((count,)),
+            dma((tp_count,)),
+            dma((tp_count,)),
             dma,
         ],
         compiler_params=pltpu.CompilerParams(collective_id=call_id, has_side_effects=True),
@@ -607,10 +688,8 @@
     return run_acc / run_total[:, None]
 
 
-def spread_shards(shard, tp_count):
-    across = lax.ppermute(shard, "tp", [(i, i ^ 2) for i in range(tp_count)])
-    beside = [(i, i ^ 1) for i in range(tp_count)]
-    return [shard, across, lax.ppermute(shard, "tp", beside), lax.ppermute(across, "tp", beside)]
+def across_pairs(shard, tp_count):
+    return lax.ppermute(shard, "tp", [(i, i ^ 2) for i in range(tp_count)])
 
 
 def slot_ranks(member):
@@ -687,21 +766,25 @@
         and tok_count % (16 * tp_count) == 0
         and entries % lanes == 0
         and head_count * tok_count % 256 == 0
+        and head_count % 2 == 0
     )
     if relayed:
-        shared_shards = [spread_shards(w, tp_count) for w in (shared_gate, shared_up, shared_down)]
+        shared_shards = []
+        for shard in (shared_gate, shared_up, shared_down):
+            shared_shards += [shard, across_pairs(shard, tp_count)]
         scale_hi = lax.reduce_precision(route_weights, 8, 7)
         tables = jnp.stack([routes.astype(jnp.float32), scale_hi, route_weights - scale_hi])
         tables = tables.astype(jnp.bfloat16).reshape(-1, lanes)
         table_rows = tables.shape[0]
         tables = jnp.pad(tables, ((0, -table_rows % 16), (0, 0)))
         scaled = rotated_query * jnp.asarray(score_scale, jnp.bfloat16)
-        everything, head_out = attend(
+        everything, token_heads = attend(
             scaled.transpose(2, 1, 0).reshape(HEAD_SIZE, head_count * tok_count),
             jnp.concatenate([packed, tables], axis=0),
             head_gain.reshape(head_count, HEAD_SIZE),
             tok_count,
             sp_count // tp_count,
+            tp_count,
             0,
         )
         tables = everything[:, tok_count : tok_count + table_rows]
@@ -715,10 +798,11 @@
         head_out = final_norm(attended, head_gain.reshape(head_count, HEAD_SIZE))
         head_out = head_out.astype(jnp.bfloat16).reshape(tok_count, head_count * HEAD_SIZE)
     part_rows = tok_count // tp_count
-    token_heads = exchange(
-        head_out.reshape(tp_count, part_rows, head_count * HEAD_SIZE), "tp", 1, False
-    )
-    token_heads = token_heads.transpose(1, 0, 2).reshape(part_rows, -1)
+    if not relayed:
+        token_heads = exchange(
+            head_out.reshape(tp_count, part_rows, head_count * HEAD_SIZE), "tp", 1, False
+        )
+        token_heads = token_heads.transpose(1, 0, 2).reshape(part_rows, -1)
     own_resid = lax.dynamic_slice_in_dim(residual, tp_index * part_rows, part_rows, 0)
     hidden_own = (
         own_resid.astype(jnp.float32)
@@ -748,25 +832,21 @@
             return table.reshape(group * capacity, tok_count)
 
         combine_hi, combine_lo = combine(1), combine(2)
-        arrived = dispatch(normed_own, select, tp_count, width, tp_count, 2)
+        arrived, *others = dispatch(
+            normed_own, select, shared_shards, tp_count, width, tp_count, 2
+        )
         produced = expert_block(
             arrived.reshape(sp_count * capacity, model_width), gate_local, up_local, down_local
         )
-        gates, ups, downs = shared_shards
-        gate_part = jnp.dot(
-            normed_own, jnp.concatenate(gates, axis=1), preferred_element_type=jnp.float32
-        )
-        up_part = jnp.dot(
-            normed_own, jnp.concatenate(ups, axis=1), preferred_element_type=jnp.float32
-        )
-        shared_inner = (jax.nn.silu(gate_part) * up_part).astype(jnp.bfloat16)
-        shared_out = jnp.dot(
-            shared_inner, jnp.concatenate(downs, axis=0), preferred_element_type=jnp.float32
-        )
-        routed = give_back(
+        every_shard = []
+        for i in range(0, len(shared_shards), 2):
+            every_shard += shared_shards[i : i + 2] + others[i : i + 2]
+        routed, shared_out = give_back(
             produced.reshape(sp_count, capacity, model_width),
             combine_hi,
             combine_lo,
+            normed_own,
+            every_shard,
             tp_count,
             width,
             tp_count,

time: 199 us -> 194 us (0.975)
  matrix products: 22.2 us -> 15.7 us
  starting transfers between devices: 4.01 us -> 1.76 us
  other arithmetic: 4.83 us -> 6.89 us
  Pallas kernels: 161 us -> 163 us
    dot_general x3 -> x1, matrix products: 11.6 us -> 5 us  [expert_block(): up_out = jnp.dot(flat_rows, up_local, preferred_element_type=jnp.float32)]
    pallas_call x1, Pallas kernels: 25.5 us -> 31.5 us  [attend(): pl.pallas_call(kernel, out_shape=(jax.ShapeDtypeStruct((count,) + own.sha...]
    pallas_call x3 -> x2, Pallas kernels: 135 us -> 131 us  [the longest x1 73.9 us: give_back(): pl.pallas_call(kernel, out_shape=(jax.ShapeDtypeStruct((rows, model), jnp...]
    ppermute x9 -> x3, starting transfers between devices: 4.01 us -> 1.76 us  [across_pairs(): return lax.ppermute(shard, 'tp', [(i, i ^ 2) for i in range(tp_count)])]
  transfers between devices with their start and end apart: 9 -> 3, of which waited for: 0 -> 0; matrix products, arithmetic and copies ran while one was open for 15% -> 7% of each run, Pallas kernels for 81% -> 16%
where the time goes in v4:
time: 194 us
  Pallas kernels  163 us (84%)
  matrix products  15.7 us (8%)
  other arithmetic  6.89 us (4%)
  local copies, waits for them, and re-layouts  6.77 us (3%)
    pallas_call x1, Pallas kernels, give_back(): pl.pallas_call(kernel, out_shape=(jax.ShapeDtypeStruct((rows, model), jnp...  73.9 us
    pallas_call x1, Pallas kernels, dispatch(): pl.pallas_call(kernel, out_shape=[jax.ShapeDtypeStruct((planes * width, c...  57.3 us
    pallas_call x1, Pallas kernels, attend(): pl.pallas_call(kernel, out_shape=(jax.ShapeDtypeStruct((count,) + own.sha...  31.5 us
    dot_general x1, matrix products, expert_block(): jnp.dot(expert_inner, down_local, preferred_element_type=jnp.float32)  7.28 us
    dot_general x1, matrix products, expert_block(): up_out = jnp.dot(flat_rows, up_local, preferred_element_type=jnp.float32)  5 us
  transfers between devices with their start and end apart: 3, of which 0 were waited for; matrix products, arithmetic and copies ran while one was open for 7% of the time, Pallas kernels for 16%

profile of v4, /device:TPU:13, one launch (start us, length us, event | category | flops | bytes accessed | tf_op | source)
XLA Modules:
  0.0 194.1 jit_solution(2703454892424372757)
XLA Ops:
  0.0 0.0 copy-start
  0.0 0.3 collective-permute-start
  0.3 1.2 collective-permute-start.1
  1.6 0.2 collective-permute-start.2
  1.8 0.7 mul.242
  2.6 1.1 copy.29
  3.6 0.0 copy-start.7
  3.6 0.1 bitcast_reduce_fusion
  3.7 0.1 fusion.26
  3.8 0.2 fusion.25
  4.0 0.1 multiply_multiply_fusion
  4.1 0.1 subtract_convert_fusion
  4.2 0.2 copy.38
  4.4 0.8 reshape.409.q_ref
  5.3 0.2 copy.33
  5.5 0.3 convert_element_type.104
  5.8 0.1 copy.32
  6.0 0.1 fusion.18
  6.1 0.2 subtract_convert_fusion.1
  6.3 0.1 copy.31
  6.5 0.7 reshape.411.gain_ref
  7.1 0.7 fusion.19.own_ref
  7.9 31.5 %attend.1 = (bf16[8,352,128]{2,1,0:T(8,128)(2,1)}, bf16[80,1024]{1,0:T(8,128)(2,1)}) custom-call(bf16[64,1280]{1,0:T(8,128)(2,1)} %reshape.409.q_ref, bf16[352,128]{1,0:T(8,128)(2,1)} %fusion.19.own_ref, f32[4,64]{1,0:T(4,128)} %reshape.411.gain_ref), custom_call_target="tpu_custom_call" | custom-call | tf_op jit(solution)/shard_map/attend/pallas_call | solution.py:633
  39.4 3.3 %multiply_reduce_fusion = (f32[80]{0:T(128)S(1)}, f32[80,2048]{1,0:T(8,128)S(1)}) fusion(bf16[80,1024]{1,0:T(8,128)(2,1)} %get-tuple-element.16, bf16[1024,2048]{1,0:T(8,128)(2,1)} %param.23, bf16[320,2048]{1,0:T(8,128)(2,1)} %param.24, s32[]{:T(128)S(6)} %select_n.56), kind=kOutput, calls=%fused_computation.20 | convolution fusion | flops 336527296 | bytes 5341508 | tf_op jit(solution)/shard_map/dot_general | solution.py:809
  42.6 0.0 copy-start.4
  42.7 0.8 slice.34
  43.5 0.2 convert_element_type.110
  43.7 0.1 copy.34
  43.8 0.1 compare_reduce_fusion
  43.9 0.1 fusion.7
  44.0 1.0 fusion.10.sel_ref
  45.0 0.2 broadcast_in_dim.30
  45.2 0.1 copy.36
  45.3 0.2 broadcast_in_dim.23
  45.5 0.1 copy.35
  45.5 0.1 fusion.21
  45.7 0.1 eq.51
  45.7 1.2 fusion.8
  46.9 0.8 multiply_convert_fusion.2.own_ref
  47.8 0.0 collective-permute-done.refs_1_
  47.8 0.0 collective-permute-done.1.refs_3_.refs_5_
  47.8 0.0 collective-permute-done.2.refs_5_.refs_9_
  47.8 0.8 copy-done.1
  48.6 57.3 %dispatch.1 = (bf16[8,80,2048]{2,1,0:T(8,128)(2,1)}, bf16[2048,128]{1,0:T(8,128)(2,1)}, bf16[2048,128]{1,0:T(8,128)(2,1)}, bf16[2048,128]{1,0:T(8,128)(2,1)}, bf...) custom-call(bf16[80,2048]{1,0:T(8,128)(2,1)} %multiply_convert_fusion.2.own_ref, ...), custom_call_target="tpu_custom_call" | custom-call | tf_op jit(solution)/shard_map/dispatch/pallas_call | solution.py:290
  105.9 5.0 %fusion.3 = f32[640,512]{1,0:T(8,128)} fusion(bf16[640,2048]{1,0:T(8,128)(2,1)} %bitcast.70, bf16[1,2048,512]{2,1,0:T(8,128)(2,1)} %param.29), kind=kOutput, calls=%fused_computation.5 | convolution fusion | flops 1342177280 | bytes 6029312 | tf_op jit(solution)/shard_map/dot_general | solution.py:704
  110.9 7.3 %convolution_convert_fusion = bf16[640,2048]{1,0:T(8,128)(2,1)} fusion(bf16[1,512,2048]{2,1,0:T(8,128)(2,1)S(1)} %copy-done, f32[640,512]{1,0:T(8,128)} %fusion.3, bf16[640,2048]{1,0:T(8,128)(2,1)} %bitcast.71, bf16[1,2048,512]{2,1,0:T(8,128)(2,1)} %param.28), kind=kOutput, calls=%fused_computation | convolution fusion | flops 2687631360 | bytes 10747904 | tf_op jit(solution)/shard_map/dot_general | solution.py:706
  118.2 73.9 %give_back.1 = (bf16[80,2048]{1,0:T(8,128)(2,1)}, f32[80,2048]{1,0:T(8,128)}) custom-call(bf16[8,80,2048]{2,1,0:T(8,128)(2,1)} %bitcast.60, bf16[640,320]{1,0:T(8,128)(2,1)} %get-tuple-element.36.hi_ref, bf16[640,320]{1,0:T(8,128)(2,1)} %get-tuple-element.35.lo_ref, bf16[80,2048]{1,0:T(8,128)(2,1)} %multiply_convert_fusion.2.own_ref, ...), custom_call_target="tpu_custom_call" | custom-call | tf_op jit(solution)/shard_map/give_back/pallas_call | solution.py:472
  192.1 2.0 %add_convert_fusion = bf16[80,2048]{1,0:T(8,128)(2,1)} fusion(f32[80,2048]{1,0:T(8,128)S(1)} %get-tuple-element.49, f32[80,2048]{1,0:T(8,128)} %get-tuple-element.25, bf16[80,2048]{1,0:T(8,128)(2,1)} %get-tuple-element.26), kind=kLoop, calls=%fused_computation.17 | loop fusion | flops 655360 | bytes 1966080 | tf_op jit(solution)/shard_map/convert_element_type | solution.py:857
  (29 shorter events, 0.2 us)
Async XLA Ops:
  0.0 110.9 %copy-start = (bf16[1,512,2048]{2,1,0:T(8,128)(2,1)S(1)}, bf16[1,512,2048]{2,1,0:T(8,128)(2,1)}, u32[]{:S(2)}) copy-start(bf16[1,512,2048]{2,1,0:T(8,128)(2,1)} %param.30) | copy-start | bytes 6291460
  0.0 5.2 %copy-start.5 = (f32[320,4]{0,1:T(4,128)S(1)}, f32[320,4]{0,1:T(4,128)}, u32[]{:S(2)}) copy-start(f32[320,4]{0,1:T(4,128)} %param.27) | copy-start | bytes 15364
  0.0 5.2 %copy-start.6 = (s32[320,4]{0,1:T(4,128)S(1)}, s32[320,4]{0,1:T(4,128)}, u32[]{:S(2)}) copy-start(s32[320,4]{0,1:T(4,128)} %param.26) | copy-start | bytes 15364
  0.0 5.8 %copy-start.3 = (bf16[320,64]{0,1:T(8,128)(2,1)S(1)}, bf16[320,64]{0,1:T(8,128)(2,1)}, u32[]{:S(2)}) copy-start(bf16[320,64]{0,1:T(8,128)(2,1)} %param.19) | copy-start | bytes 122884
  0.0 5.9 %copy-start.2 = (bf16[320,64]{0,1:T(8,128)(2,1)S(1)}, bf16[320,64]{0,1:T(8,128)(2,1)}, u32[]{:S(2)}) copy-start(bf16[320,64]{0,1:T(8,128)(2,1)} %param.18) | copy-start | bytes 122884
  0.0 6.0 %copy-start.8 = (f32[64]{0:T(128)S(1)}, f32[64]{0:T(128)}, u32[]{:S(2)}) copy-start(f32[64]{0:T(128)} %param.21) | copy-start | bytes 772
  0.0 47.8 %collective-permute-start = (bf16[2048,128]{1,0:T(8,128)(2,1)}, bf16[2048,128]{1,0:T(8,128)(2,1)S(1)}, u32[]{:S(2)}, u32[]{:S(2)}) collective-permute-start(bf16[2048,128]{1,0:T(8,128)(2,1)} %refs_0_.3), channel_id=1, source_target_pairs={{0,2},{1,3},{2,0},{3,1},{4,6},{5,7},{6,4},{7,5},{8,10},{9,11},{10,... | collective-permute-start | bytes 1572872 | tf_op jit(solution)/shard_map/ppermute | solution.py:692
  0.3 47.5 %collective-permute-start.1 = (bf16[2048,128]{1,0:T(8,128)(2,1)}, bf16[2048,128]{1,0:T(8,128)(2,1)}, u32[]{:S(2)}, u32[]{:S(2)}) collective-permute-start(bf16[2048,128]{1,0:T(8,128)(2,1)} %refs_4_.3), channel_id=1, source_target_pairs={{0,2},{1,3},{2,0},{3,1},{4,6},{5,7},{6,4},{7,5},{8,10},{9,11},{10,... | collective-permute-start | bytes 1572872 | tf_op jit(solution)/shard_map/ppermute | solution.py:692
  1.6 46.2 %collective-permute-start.2 = (bf16[128,2048]{1,0:T(8,128)(2,1)}, bf16[128,2048]{1,0:T(8,128)(2,1)}, u32[]{:S(2)}, u32[]{:S(2)}) collective-permute-start(bf16[128,2048]{1,0:T(8,128)(2,1)} %refs_8_.1), channel_id=1, source_target_pairs={{0,2},{1,3},{2,0},{3,1},{4,6},{5,7},{6,4},{7,5},{8,10},{9,11},{10,... | collective-permute-start | bytes 1572872 | tf_op jit(solution)/shard_map/ppermute | solution.py:692
  3.6 2.8 %copy-start.7 = (f32[256]{0:T(256)S(1)}, f32[256]{0:T(256)}, u32[]{:S(2)}) copy-start(f32[256]{0:T(256)} %param.22) | copy-start | bytes 3076
  42.6 4.3 %copy-start.4 = (f32[2048]{0:T(1024)S(1)}, f32[2048]{0:T(1024)}, u32[]{:S(2)}) copy-start(f32[2048]{0:T(1024)} %param.25) | copy-start | bytes 24580
  47.8 0.8 copy-start.1
